TPU v7x, 256 devices: a whole 4x4x8 slice. The times are simulated.
256 devices in a mesh: sp: 16 (over y, x), tp: 16 (over z, core).
Axes of the slice: x: 4, y: 4, z: 8, core: 2. Of those that a mesh axis runs over, the one named last changes fastest.
Arguments:
- upstream: bfloat16 [4096, 4096], P('sp', 'tp'), may hold values from -6 to 6
- stream: bfloat16 [4096, 4096], P('sp', 'tp'), may hold values from -400 to 400
- norm_gain: float32 [4096], P('tp'), may hold values from 0.1 to 1.9
- routes: int32 [4096, 2], P('sp'), may hold values from 0 to 15, all different within a row; in each aligned block of 256 rows (0 to 255, 256 to 511, ...) at most 48 rows name the same one
- route_weights: float32 [4096, 2], P('sp'), may hold values from 0.1 to 1
- w_gate: bfloat16 [16, 4096, 2048], P('sp', None, 'tp'), may hold values from -0.09375 to 0.09375
- w_up: bfloat16 [16, 4096, 2048], P('sp', None, 'tp'), may hold values from -0.09375 to 0.09375
- w_down: bfloat16 [16, 2048, 4096], P('sp', 'tp'), may hold values from -0.125 to 0.125
- value_in: bfloat16 [4096, 2048], P('sp', 'tp'), may hold values from -6 to 6
- gate_in: bfloat16 [4096, 2048], P('sp', 'tp'), may hold values from -6 to 6
- conv_pre: bfloat16 [4096, 2048], P('sp', 'tp'), may hold values from -200 to 200
- ln_gain: float32 [2048], P('tp'), may hold values from 0.1 to 1.9
- conv_taps: float32 [31, 2048], P(None, 'tp'), may hold values from -1 to 1
- w_out: bfloat16 [2048, 4096], P('tp'), may hold values from -0.125 to 0.125
Outputs:
- grad_gate: float32 [16, 4096, 2048], P('sp', None, 'tp')
- grad_up: float32 [16, 4096, 2048], P('sp', None, 'tp')
- grad_down: float32 [16, 2048, 4096], P('sp', 'tp')
- grad_out: float32 [2048, 4096], P('tp', 'sp')
- value_grad: bfloat16 [4096, 2048], P('sp', 'tp')
- gate_grad: bfloat16 [4096, 2048], P('sp', 'tp')
Inputs may be any that keep to these rules, and one draw needn't show every extreme that they name: `routes`: each token names two different experts. Among the tokens of one index of sp no expert is named more than 48 times, and in every draw some expert exactly 48 times.
All inputs are finite; a program needn't handle non-finite values.
Results may differ from a plain program's by a relative error of at most 0.0071.
Values may be sent and summed in bfloat16 or wider, within the bound.
A program may use at most 128 MiB of HBM per device.

v0:
```python
import jax
import jax.numpy as jnp
from jax import lax
from jax.sharding import PartitionSpec as P

EPSILON = 1e-06


def sent_to_all(value, axis):
    count = lax.axis_size(axis)
    return lax.all_to_all(
        jnp.broadcast_to(value[None], (count, *value.shape)), axis, 0, 0, tiled=True
    )


def of_everyone(value, axis):
    everything = sent_to_all(value, axis)
    return jnp.sum(everything, axis=0)


def in_one(arrays, axis):
    vector, at, gathered = (jnp.concatenate([a.reshape(-1) for a in arrays]), 0, [])
    total = of_everyone(vector, axis)
    for a in arrays:
        gathered.append(total[at : at + a.size].reshape(a.shape))
        at += a.size
    return tuple(gathered)


def side_by_side(arrays, axis, split_dim, concat_dim, along):
    both = jnp.concatenate(arrays, axis=along)
    out, at, gathered = (
        lax.all_to_all(both, axis, split_axis=split_dim, concat_axis=concat_dim, tiled=True),
        0,
        [],
    )
    for a in arrays:
        gathered.append(lax.slice_in_dim(out, at, at + a.shape[along], axis=along))
        at += a.shape[along]
    return tuple(gathered)


def in_one_piece(arrays, axis, dim, along):
    widths = [a.shape[along] for a in arrays]
    both = jnp.concatenate(arrays, axis=along)
    out = lax.all_gather(both, axis, axis=dim, tiled=True)
    return tuple(jnp.split(out, [sum(widths[:k]) for k in range(1, len(widths))], axis=along))


def cut_along(value, dim, count):
    shape = value.shape
    blocks = value.reshape(*shape[:dim], count, shape[dim] // count, *shape[dim + 1 :])
    return jnp.moveaxis(blocks, dim, 0)


def sent_and_summed(value, axis, dim):
    count = lax.axis_size(axis)
    blocks = lax.all_to_all(cut_along(value, dim, count), axis, 0, 0, tiled=True)
    return jnp.sum(blocks.astype(jnp.float32), axis=0)


def shifted(block, axis, distance):
    devices = range(lax.axis_size(axis))
    route = [(i - distance, i) for i in devices if i - distance in devices]
    return lax.ppermute(block, axis, route)


def silu_slope(values):
    logistic = jax.nn.sigmoid(values)
    return logistic * (1.0 + values * (1.0 - logistic))


def per_device(
    upstream,
    stream,
    norm_gain,
    routes,
    route_weights,
    w_gate,
    w_up,
    w_down,
    value_in,
    gate_in,
    conv_pre,
    ln_gain,
    conv_taps,
    w_out,
):
    tok_rows, width_part = stream.shape
    token_groups = lax.axis_size("sp")
    width_groups = lax.axis_size("tp")
    model_width = width_part * width_groups
    channels = conv_pre.shape[1] * width_groups
    tap_count = conv_taps.shape[0]
    capacity = 3 * tok_rows // token_groups
    experts = w_gate.shape[0] * token_groups
    slot_count = experts * capacity
    expert_rows = token_groups * capacity
    residual = stream.astype(jnp.float32)
    conv_vals = conv_pre.astype(jnp.float32)
    row_squares, conv_total, conv_squares = in_one(
        (
            jnp.sum(residual * residual, axis=1),
            jnp.sum(conv_vals, axis=1),
            jnp.sum(conv_vals * conv_vals, axis=1),
        ),
        "tp",
    )
    inverse = lax.rsqrt(row_squares / model_width + EPSILON)[:, None]
    normed = (norm_gain[None, :] * residual * inverse).astype(jnp.bfloat16)
    flat_experts = routes.reshape(-1)
    one_hot = (flat_experts[:, None] == jnp.arange(experts, dtype=jnp.int32)[None, :]).astype(
        jnp.int32
    )
    slot_rank = jnp.sum((jnp.cumsum(one_hot, axis=0) - one_hot) * one_hot, axis=1)
    slot_index = (flat_experts * capacity + slot_rank).reshape(tok_rows, 2)
    slot_ids = jnp.arange(slot_count, dtype=jnp.int32)[:, None]
    first_hit = slot_ids == slot_index[None, :, 0]
    second_hit = slot_ids == slot_index[None, :, 1]
    any_hit = jnp.logical_or(first_hit, second_hit)
    picker = any_hit.astype(jnp.bfloat16)
    slot_weight = jnp.sum(
        jnp.where(first_hit, route_weights[None, :, 0], 0.0)
        + jnp.where(second_hit, route_weights[None, :, 1], 0.0),
        axis=1,
    )
    token_iota = jnp.arange(tok_rows, dtype=jnp.int32)[None, :]
    slot_token = jnp.where(
        jnp.any(any_hit, axis=1), jnp.sum(jnp.where(any_hit, token_iota, 0), axis=1), tok_rows
    )
    columns = normed.shape[1]
    normed_pad = jnp.concatenate([normed, jnp.zeros((1, columns), jnp.bfloat16)], axis=0)
    upstream_pad = jnp.concatenate([upstream, jnp.zeros((1, columns), jnp.bfloat16)], axis=0)
    inputs = normed_pad[slot_token]
    cotangent = (upstream_pad[slot_token].astype(jnp.float32) * slot_weight[:, None]).astype(
        jnp.bfloat16
    )
    sent_inputs = inputs.reshape(experts, capacity, columns)
    sent_cotangent = cotangent.reshape(experts, capacity, columns)
    part_inputs, part_cotangent = side_by_side((sent_inputs, sent_cotangent), "sp", 0, 0, 1)
    inputs, cotangent = in_one_piece(
        (
            part_inputs.reshape(expert_rows, width_part),
            part_cotangent.reshape(expert_rows, width_part),
        ),
        "tp",
        1,
        0,
    )
    gate_mat = w_gate[0]
    upper_mat = w_up[0]
    down_mat = w_down[0]
    gate_pre = jnp.dot(inputs, gate_mat, preferred_element_type=jnp.float32)
    upper_pre = jnp.dot(inputs, upper_mat, preferred_element_type=jnp.float32)
    active = (jax.nn.silu(gate_pre) * upper_pre).astype(jnp.bfloat16)
    active_back = lax.dot_general(
        cotangent, down_mat, (((1,), (1,)), ((), ())), preferred_element_type=jnp.float32
    )
    gate_back = (active_back * upper_pre * silu_slope(gate_pre)).astype(jnp.bfloat16)
    upper_back = (active_back * jax.nn.silu(gate_pre)).astype(jnp.bfloat16)
    grad_gate = lax.dot_general(
        inputs, gate_back, (((0,), (0,)), ((), ())), preferred_element_type=jnp.float32
    )
    grad_up = lax.dot_general(
        inputs, upper_back, (((0,), (0,)), ((), ())), preferred_element_type=jnp.float32
    )
    grad_down = lax.dot_general(
        active, cotangent, (((0,), (0,)), ((), ())), preferred_element_type=jnp.float32
    )
    input_part = lax.dot_general(
        gate_back, gate_mat, (((1,), (1,)), ((), ())), preferred_element_type=jnp.float32
    ) + lax.dot_general(
        upper_back, upper_mat, (((1,), (1,)), ((), ())), preferred_element_type=jnp.float32
    )
    input_back = lax.psum_scatter(
        input_part.astype(jnp.bfloat16), "tp", scatter_dimension=1, tiled=True
    )
    returned = lax.all_to_all(
        input_back.reshape(token_groups, capacity, width_part),
        "sp",
        split_axis=0,
        concat_axis=0,
        tiled=True,
    )
    returned = returned.reshape(slot_count, width_part)
    token_back = lax.dot_general(
        picker, returned, (((0,), (0,)), ((), ())), preferred_element_type=jnp.float32
    )
    gained = norm_gain[None, :] * token_back
    inner_sum = of_everyone(jnp.sum(gained * residual, axis=1), "tp")
    norm_back = inverse * gained - residual * inverse**3 * (inner_sum / model_width)[:, None]
    stream_grad = (upstream.astype(jnp.float32) + norm_back).astype(jnp.bfloat16)
    full_grad = lax.all_gather(stream_grad, "tp", axis=1, tiled=True)
    mean_val = (conv_total / channels)[:, None]
    variance = (conv_squares / channels)[:, None] - mean_val * mean_val
    inv_std = lax.rsqrt(variance + EPSILON)
    centred = (conv_vals - mean_val) * inv_std
    scaled = centred * ln_gain[None, :]
    mixed_out = jax.nn.silu(scaled).astype(jnp.bfloat16)
    columns = full_grad
    grad_rows = sent_and_summed(
        lax.dot_general(
            columns, mixed_out, (((0,), (0,)), ((), ())), preferred_element_type=jnp.float32
        ).astype(jnp.bfloat16),
        "sp",
        0,
    )
    grad_out = grad_rows.T
    mixed_back = lax.dot_general(
        full_grad, w_out, (((1,), (1,)), ((), ())), preferred_element_type=jnp.float32
    )
    norm_in = mixed_back * silu_slope(scaled) * ln_gain[None, :]
    norm_total, norm_cross = in_one(
        (jnp.sum(norm_in, axis=1), jnp.sum(norm_in * centred, axis=1)), "tp"
    )
    conv_back = inv_std * (
        norm_in - (norm_total / channels)[:, None] - centred * (norm_cross / channels)[:, None]
    )
    next_rim = shifted(conv_back[: tap_count - 1], "sp", -1)
    padded = jnp.concatenate([conv_back, next_rim], axis=0)
    glu_back = jnp.zeros(conv_back.shape, jnp.float32)
    for tap_index in range(tap_count):
        offset = tap_count - 1 - tap_index
        glu_back = glu_back + conv_taps[tap_index][None, :] * padded[offset : offset + tok_rows]
    gate_sigma = jax.nn.sigmoid(gate_in.astype(jnp.float32))
    value_grad = (glu_back * gate_sigma).astype(jnp.bfloat16)
    gate_grad = (glu_back * value_in.astype(jnp.float32) * gate_sigma * (1.0 - gate_sigma)).astype(
        jnp.bfloat16
    )
    return (grad_gate[None], grad_up[None], grad_down[None], grad_out, value_grad, gate_grad)


def solution(mesh):
    return jax.shard_map(
        per_device,
        mesh=mesh,
        in_specs=(
            P("sp", "tp"),
            P("sp", "tp"),
            P("tp"),
            P("sp", None),
            P("sp", None),
            P("sp", None, "tp"),
            P("sp", None, "tp"),
            P("sp", "tp", None),
            P("sp", "tp"),
            P("sp", "tp"),
            P("sp", "tp"),
            P("tp"),
            P(None, "tp"),
            P("tp", None),
        ),
        out_specs=(
            P("sp", None, "tp"),
            P("sp", None, "tp"),
            P("sp", "tp", None),
            P("tp", "sp"),
            P("sp", "tp"),
            P("sp", "tp"),
        ),
        check_vma=False,
    )
```

profile of v0, /device:TPU:17, one launch (start us, length us, event | category | flops | bytes accessed | tf_op | source)
XLA Modules:
  0.0 323.8 jit_solution(10947476030596708137)
XLA Ops:
  7.2 1.1 copy.69
  8.3 1.0 convert_reduce_fusion.1
  9.3 0.6 broadcast_in_dim.81
  10.0 9.2 %all-to-all-start = ((f32[16,1,768]{2,1,0:T(1,128)}), f32[16,1,768]{2,1,0:T(1,128)S(1)}, u32[]{:S(2)}, u32[]{:S(2)}) async-start(f32[16,1,768]{2,1,0:T(1,128)} %broadcast_in_dim.81), calls=%async_computation | async-start | bytes 98304 | tf_op jit(solution)/shard_map/all_to_all | solution.py:11
  19.2 0.8 copy.71
  20.3 1.2 reduce-window.6
  22.0 0.7 multiply_add_fusion
  22.7 0.2 fusion.23
  23.2 0.8 fusion.157
  24.0 0.2 add_reduce_fusion
  24.3 0.9 concatenate.23
  25.2 2.7 gather_fusion.1
  28.1 0.6 slice_multiply_fusion.2
  28.7 0.8 fusion.28
  29.6 2.7 gather_fusion
  32.4 18.3 %all_to_all.33 = bf16[16,96,256]{2,1,0:T(8,128)(2,1)S(1)} all-to-all(bf16[16,96,256]{2,1,0:T(8,128)(2,1)S(1)} %pad_maximum_fusion), channel_id=1, replica_groups=mesh['sp'=16,'tp'=16] {'sp'}, dimensions={0} | all-to-all | bytes 1572864 | tf_op jit(solution)/shard_map/all_to_all | solution.py:33
  50.7 0.9 pad_maximum_fusion.1
  51.9 82.0 %all-gather.3.cloned.1.call-done = bf16[1536,4096]{1,0:T(8,128)(2,1)} async-done(((bf16[1536,256]{1,0:T(8,128)(2,1)}), bf16[1536,4096]{1,0:T(8,128)(2,1)}) %all-gather.3.cloned.1.call-update) | async-done | bytes 12582928 | tf_op jit(solution)/shard_map/all_gather | solution.py:46
  133.9 4.7 %fusion.9 = f32[768,128]{1,0:T(8,128)S(1)} fusion(bf16[1536,4096]{1,0:T(8,128)(2,1)} %all-gather.3.cloned.1.call-done, bf16[1,4096,128]{2,1,0:T(8,128)(2,1)S(1)} %copy-done), kind=kOutput, calls=%fused_computation.13 | convolution fusion | flops 805306368 | bytes 7733248 | tf_op jit(solution)/shard_map/dot_general | solution.py:153
  138.7 5.2 %fusion.11 = f32[768,128]{1,0:T(8,128)S(1)} fusion(bf16[1536,4096]{1,0:T(8,128)(2,1)} %all-gather.3.cloned.1.call-done, bf16[1,4096,128]{2,1,0:T(8,128)(2,1)S(1)} %copy-done.2), kind=kOutput, calls=%fused_computation.15 | convolution fusion | flops 805306368 | bytes 7733248 | tf_op jit(solution)/shard_map/dot_general | solution.py:154
  143.9 1.8 multiply_convert_fusion.1
  145.7 1.8 fusion.14
  147.5 4.4 %add_convert_fusion = bf16[768,4096]{1,0:T(8,128)(2,1)} fusion(f32[768,4096]{1,0:T(8,128)S(1)} %fusion.14, bf16[768,128]{1,0:T(8,128)(2,1)S(1)} %get-tuple-element.36, bf16[1,4096,128]{2,1,0:T(8,128)(2,1)S(1)} %copy-done.2), kind=kOutput, calls=%fused_computation.2 | convolution fusion | flops 811597824 | bytes 20119552 | tf_op jit(solution)/shard_map/dot_general | solution.py:172
  152.0 61.8 %reduce-scatter.2.cloned.1.call-done = bf16[768,256]{1,0:T(8,128)(2,1)} async-done(((bf16[768,4096]{1,0:T(8,128)(2,1)}), bf16[768,256]{1,0:T(8,128)(2,1)}) %reduce-scatter.2.cloned.1.call-update) | async-done | bytes 393232 | tf_op jit(solution)/shard_map/reduce_scatter | solution.py:175
  213.8 12.6 %all_to_all.34 = bf16[16,48,256]{2,1,0:T(8,128)(2,1)S(1)} all-to-all(bf16[16,48,256]{2,1,0:T(8,128)(2,1)} %bitcast.128), channel_id=1, replica_groups=mesh['sp'=16,'tp'=16] {'sp'}, dimensions={0} | all-to-all | bytes 786432 | tf_op jit(solution)/shard_map/all_to_all | solution.py:178
  226.4 0.4 fusion.34
  226.8 0.6 broadcast_in_dim.93
  227.5 9.6 %all-to-all-start.3 = ((f32[16,1,256]{2,1,0:T(1,128)}), f32[16,1,256]{2,1,0:T(1,128)S(1)}, u32[]{:S(2)}, u32[]{:S(2)}) async-start(f32[16,1,256]{2,1,0:T(1,128)} %broadcast_in_dim.93), calls=%async_computation.4 | async-start | bytes 32768 | tf_op jit(solution)/shard_map/all_to_all | solution.py:11
  237.1 0.3 all-gather.5.cloned.1.call-start
  237.4 7.0 %all-to-all-done.3 = f32[16,1,256]{2,1,0:T(1,128)S(1)} async-done(((f32[16,1,256]{2,1,0:T(1,128)}), f32[16,1,256]{2,1,0:T(1,128)S(1)}, u32[]{:S(2)}, u32[]{:S(2)}) %all-to-all-start.3) | async-done | bytes 16416 | tf_op jit(solution)/shard_map/all_to_all | solution.py:11
  244.4 0.7 fusion.33
  245.2 0.5 slice_bitcast_fusion.29
  245.7 0.7 slice_bitcast_fusion.30
  246.4 5.9 %convolution_bitcast_fusion.1 = f32[1,4096,128]{2,1,0:T(8,128)} fusion(bf16[768,128]{1,0:T(8,128)(2,1)S(1)} %get-tuple-element.37, bf16[1536,4096]{1,0:T(8,128)(2,1)} %all-gather.3.cloned.1.call-done), kind=kOutput, calls=%fused_computation.9 | convolution fusion | flops 805306368 | bytes 8585216 | tf_op jit(solution)/shard_map/dot_general | solution.py:161
  252.4 6.0 %convolution_bitcast_fusion = f32[1,4096,128]{2,1,0:T(8,128)} fusion(bf16[768,128]{1,0:T(8,128)(2,1)S(1)} %get-tuple-element.36, bf16[1536,4096]{1,0:T(8,128)(2,1)} %all-gather.3.cloned.1.call-done), kind=kOutput, calls=%fused_computation.8 | convolution fusion | flops 805306368 | bytes 8585216 | tf_op jit(solution)/shard_map/dot_general | solution.py:164
  258.4 21.2 %all-gather.5.cloned.1.call-done = bf16[256,4096]{0,1:T(8,128)(2,1)} async-done(((bf16[256,256]{0,1:T(8,128)(2,1)}), bf16[256,4096]{0,1:T(8,128)(2,1)}) %all-gather.5.cloned.1.call-update) | async-done | bytes 2097168 | tf_op jit(solution)/shard_map/all_gather | solution.py:193
  279.6 2.5 fusion.154
  282.1 0.6 broadcast_in_dim.94
  282.7 4.4 %all-to-all-start.5 = ((f32[16,1,512]{2,1,0:T(1,128)}), f32[16,1,512]{2,1,0:T(1,128)S(1)}, u32[]{:S(2)}, u32[]{:S(2)}) async-start(f32[16,1,512]{2,1,0:T(1,128)} %broadcast_in_dim.94), calls=%async_computation.6 | async-start | bytes 65536 | tf_op jit(solution)/shard_map/all_to_all | solution.py:11
  287.1 3.4 %convolution_convert_fusion = bf16[4096,128]{1,0:T(8,128)(2,1)} fusion(bf16[256,4096]{0,1:T(8,128)(2,1)} %all-gather.5.cloned.1.call-done, bf16[256,128]{1,0:T(8,128)(2,1)S(1)} %copy-done.3, f32[128]{0:T(128)S(1)} %copy-done.36, f32[256]{0:T(256)S(1)} %copy-done.9, f32[256]{0:T(256)S(1)} %copy-done.8), kind=kOutput, calls=%fused_computation.10 | convolution fusion | flops 269254656 | bytes 3213824 | tf_op jit(solution)/shard_map/dot_general | solution.py:202
  290.7 3.8 %all-to-all-done.5 = f32[16,1,512]{2,1,0:T(1,128)S(1)} async-done(((f32[16,1,512]{2,1,0:T(1,128)}), f32[16,1,512]{2,1,0:T(1,128)S(1)}, u32[]{:S(2)}, u32[]{:S(2)}) %all-to-all-start.5) | async-done | bytes 32800 | tf_op jit(solution)/shard_map/all_to_all | solution.py:11
  294.5 6.7 %all-to-all-start.4 = ((bf16[16,256,128]{2,1,0:T(8,128)(2,1)}), bf16[16,256,128]{2,1,0:T(8,128)(2,1)S(1)}, u32[]{:S(2)}, u32[]{:S(2)}) async-start(bf16[16,256,128]{2,1,0:T(8,128)(2,1)} %bitcast.17), calls=%async_computation.5 | async-start | bytes 2097152 | tf_op jit(solution)/shard_map/all_to_all | solution.py:58
  301.4 4.3 %collective-permute-start = (f32[30,128]{1,0:T(8,128)S(1)}, f32[30,128]{1,0:T(8,128)S(1)}, u32[]{:S(2)}, u32[]{:S(2)}) collective-permute-start(f32[30,128]{1,0:T(8,128)S(1)} %slice.309), channel_id=1, source_target_pairs={{16,0},{32,16},{48,32},{64,48},{80,64},{96,80},{112,96},{128,112},... | collective-permute-start | bytes 46088 | tf_op jit(solution)/shard_map/ppermute | solution.py:65
  305.8 5.2 %fusion.4 = f32[1,128,4096]{2,1,0:T(8,128)} fusion(bf16[1536,4096]{1,0:T(8,128)(2,1)} %all-gather.3.cloned.1.call-done, f32[768,128]{1,0:T(8,128)S(1)} %fusion.11, f32[768,128]{1,0:T(8,128)S(1)} %fusion.9), kind=kOutput, calls=%fused_computation.7 | convolution fusion | flops 805896192 | bytes 9175040 | tf_op jit(solution)/shard_map/dot_general | solution.py:167
  310.9 3.4 %collective-permute-done = f32[30,128]{1,0:T(8,128)S(1)} collective-permute-done((f32[30,128]{1,0:T(8,128)S(1)}, f32[30,128]{1,0:T(8,128)S(1)}, u32[]{:S(2)}, u32[]{:S(2)}) %collective-permute-start) | collective-permute-done | bytes 15392 | tf_op jit(solution)/shard_map/ppermute | solution.py:65
  314.6 1.1 multiply_convert_fusion.4
  315.7 0.7 multiply_convert_fusion.5
  316.6 0.8 copy.79
  (117 shorter events, 2.7 us)
Async XLA Ops:
  7.2 126.7 %copy-start = (bf16[1,4096,128]{2,1,0:T(8,128)(2,1)S(1)}, bf16[1,4096,128]{2,1,0:T(8,128)(2,1)}, u32[]{:S(2)}) copy-start(bf16[1,4096,128]{2,1,0:T(8,128)(2,1)} %param.19) | copy-start | bytes 3145732
  10.0 18.1 %all-to-all-start = ((f32[16,1,768]{2,1,0:T(1,128)}), f32[16,1,768]{2,1,0:T(1,128)S(1)}, u32[]{:S(2)}, u32[]{:S(2)}) async-start(f32[16,1,768]{2,1,0:T(1,128)} %broadcast_in_dim.81), calls=%async_computation | async-start | bytes 98304 | tf_op jit(solution)/shard_map/all_to_all | solution.py:11
  19.1 114.8 %all-gather.3.cloned.1.call-start = ((), (), s32[]{:S(2)}) async-start(), calls=%async_computation.7 | async-start | bytes 13369344 | tf_op jit(solution)/shard_map/all_gather | solution.py:46
  50.7 87.9 %copy-start.2 = (bf16[1,4096,128]{2,1,0:T(8,128)(2,1)S(1)}, bf16[1,4096,128]{2,1,0:T(8,128)(2,1)}, u32[]{:S(2)}) copy-start(bf16[1,4096,128]{2,1,0:T(8,128)(2,1)} %param.20) | copy-start | bytes 3145732
  51.7 162.1 %reduce-scatter.2.cloned.1.call-start = ((), (), s32[]{:S(2)}) async-start(), calls=%async_computation.8 | async-start | bytes 6684672 | tf_op jit(solution)/shard_map/reduce_scatter | solution.py:175
  133.9 10.0 %copy-start.1 = (bf16[1536,4096]{1,0:T(8,128)(2,1)S(1)}, bf16[1536,4096]{1,0:T(8,128)(2,1)}, u32[]{:S(2)}) copy-start(bf16[1536,4096]{1,0:T(8,128)(2,1)} %all-gather.3.cloned.1.call-done) | copy-start | bytes 37748740
  138.6 5.3 %copy-start.37 = (bf16[1,128,4096]{2,1,0:T(8,128)(2,1)S(1)}, bf16[1,128,4096]{2,1,0:T(8,128)(2,1)}, u32[]{:S(2)}) copy-start(bf16[1,128,4096]{2,1,0:T(8,128)(2,1)} %param.21) | copy-start | bytes 3145732
  152.0 74.5 %copy-start.35 = (f32[256]{0:T(256)S(1)}, f32[256]{0:T(256)}, u32[]{:S(2)}) copy-start(f32[256]{0:T(256)} %param.16) | copy-start | bytes 3076
  152.0 85.4 %copy-start.4 = (bf16[256,256]{1,0:T(8,128)(2,1)S(1)}, bf16[256,256]{1,0:T(8,128)(2,1)}, u32[]{:S(2)}) copy-start(bf16[256,256]{1,0:T(8,128)(2,1)} %param.14) | copy-start | bytes 393220
  152.0 92.5 %copy-start.10 = (f32[256]{0:T(256)S(1)}, f32[256]{0:T(256)}, u32[]{:S(2)}) copy-start(f32[256]{0:T(256)} %get-tuple-element.72) | copy-start | bytes 3076
  152.0 93.2 %copy-start.7 = (f32[31,128]{1,0:T(8,128)S(1)}, f32[31,128]{1,0:T(8,128)}, u32[]{:S(2)}) copy-start(f32[31,128]{1,0:T(8,128)} %param.26) | copy-start | bytes 47620
  227.5 16.9 %all-to-all-start.3 = ((f32[16,1,256]{2,1,0:T(1,128)}), f32[16,1,256]{2,1,0:T(1,128)S(1)}, u32[]{:S(2)}, u32[]{:S(2)}) async-start(f32[16,1,256]{2,1,0:T(1,128)} %broadcast_in_dim.93), calls=%async_computation.4 | async-start | bytes 32768 | tf_op jit(solution)/shard_map/all_to_all | solution.py:11
  237.1 42.5 %all-gather.5.cloned.1.call-start = ((), (), s32[]{:S(2)}) async-start(), calls=%async_computation.9 | async-start | bytes 2228224 | tf_op jit(solution)/shard_map/all_gather | solution.py:193
  252.3 27.3 %copy-start.3 = (bf16[256,128]{1,0:T(8,128)(2,1)S(1)}, bf16[256,128]{1,0:T(8,128)(2,1)}, u32[]{:S(2)}) copy-start(bf16[256,128]{1,0:T(8,128)(2,1)} %param.24) | copy-start | bytes 196612
  252.3 27.3 %copy-start.8 = (f32[256]{0:T(256)S(1)}, f32[256]{0:T(256)}, u32[]{:S(2)}) copy-start(f32[256]{0:T(256)} %get-tuple-element.71) | copy-start | bytes 3076
  252.3 27.3 %copy-start.9 = (f32[256]{0:T(256)S(1)}, f32[256]{0:T(256)}, u32[]{:S(2)}) copy-start(f32[256]{0:T(256)} %get-tuple-element.74) | copy-start | bytes 3076
  252.4 27.3 %copy-start.36 = (f32[128]{0:T(128)S(1)}, f32[128]{0:T(128)}, u32[]{:S(2)}) copy-start(f32[128]{0:T(128)} %param.25) | copy-start | bytes 1540
  252.4 27.3 %copy-start.38 = (bf16[128,4096]{1,0:T(8,128)(2,1)S(1)}, bf16[128,4096]{1,0:T(8,128)(2,1)}, u32[]{:S(2)}) copy-start(bf16[128,4096]{1,0:T(8,128)(2,1)} %param.27) | copy-start | bytes 3145732
  282.7 11.8 %all-to-all-start.5 = ((f32[16,1,512]{2,1,0:T(1,128)}), f32[16,1,512]{2,1,0:T(1,128)S(1)}, u32[]{:S(2)}, u32[]{:S(2)}) async-start(f32[16,1,512]{2,1,0:T(1,128)} %broadcast_in_dim.94), calls=%async_computation.6 | async-start | bytes 65536 | tf_op jit(solution)/shard_map/all_to_all | solution.py:11
  290.5 23.8 %copy-start.5 = (bf16[256,128]{1,0:T(8,128)(2,1)S(1)}, bf16[256,128]{1,0:T(8,128)(2,1)}, u32[]{:S(2)}) copy-start(bf16[256,128]{1,0:T(8,128)(2,1)} %param.23) | copy-start | bytes 196612
  290.5 23.8 %copy-start.6 = (bf16[256,128]{1,0:T(8,128)(2,1)S(1)}, bf16[256,128]{1,0:T(8,128)(2,1)}, u32[]{:S(2)}) copy-start(bf16[256,128]{1,0:T(8,128)(2,1)} %param.22) | copy-start | bytes 196612
  290.5 23.8 %copy-start.11 = (f32[128]{0:T(128)S(1)}, f32[128]{0:T(128)}, u32[]{:S(2)}) copy-start(f32[128]{0:T(128)} %get-tuple-element.66) | copy-start | bytes 1540
  290.5 23.8 %copy-start.12 = (f32[128]{0:T(128)S(1)}, f32[128]{0:T(128)}, u32[]{:S(2)}) copy-start(f32[128]{0:T(128)} %get-tuple-element.67) | copy-start | bytes 1540
  290.5 23.8 %copy-start.13 = (f32[128]{0:T(128)S(1)}, f32[128]{0:T(128)}, u32[]{:S(2)}) copy-start(f32[128]{0:T(128)} %get-tuple-element.68) | copy-start | bytes 1540
  290.5 23.8 %copy-start.14 = (f32[128]{0:T(128)S(1)}, f32[128]{0:T(128)}, u32[]{:S(2)}) copy-start(f32[128]{0:T(128)} %get-tuple-element.69) | copy-start | bytes 1540
  290.5 23.8 %copy-start.15 = (f32[128]{0:T(128)S(1)}, f32[128]{0:T(128)}, u32[]{:S(2)}) copy-start(f32[128]{0:T(128)} %get-tuple-element.70) | copy-start | bytes 1540
  290.6 23.8 %copy-start.16 = (f32[128]{0:T(128)S(1)}, f32[128]{0:T(128)}, u32[]{:S(2)}) copy-start(f32[128]{0:T(128)} %get-tuple-element.40) | copy-start | bytes 1540
  290.6 23.8 %copy-start.17 = (f32[128]{0:T(128)S(1)}, f32[128]{0:T(128)}, u32[]{:S(2)}) copy-start(f32[128]{0:T(128)} %get-tuple-element.41) | copy-start | bytes 1540
  290.6 23.8 %copy-start.18 = (f32[128]{0:T(128)S(1)}, f32[128]{0:T(128)}, u32[]{:S(2)}) copy-start(f32[128]{0:T(128)} %get-tuple-element.42) | copy-start | bytes 1540
  290.6 23.8 %copy-start.19 = (f32[128]{0:T(128)S(1)}, f32[128]{0:T(128)}, u32[]{:S(2)}) copy-start(f32[128]{0:T(128)} %get-tuple-element.43) | copy-start | bytes 1540
  290.6 23.8 %copy-start.20 = (f32[128]{0:T(128)S(1)}, f32[128]{0:T(128)}, u32[]{:S(2)}) copy-start(f32[128]{0:T(128)} %get-tuple-element.44) | copy-start | bytes 1540
  290.6 23.8 %copy-start.21 = (f32[128]{0:T(128)S(1)}, f32[128]{0:T(128)}, u32[]{:S(2)}) copy-start(f32[128]{0:T(128)} %get-tuple-element.45) | copy-start | bytes 1540
  290.6 23.8 %copy-start.22 = (f32[128]{0:T(128)S(1)}, f32[128]{0:T(128)}, u32[]{:S(2)}) copy-start(f32[128]{0:T(128)} %get-tuple-element.46) | copy-start | bytes 1540
  290.6 23.8 %copy-start.23 = (f32[128]{0:T(128)S(1)}, f32[128]{0:T(128)}, u32[]{:S(2)}) copy-start(f32[128]{0:T(128)} %get-tuple-element.47) | copy-start | bytes 1540
  290.6 23.8 %copy-start.24 = (f32[128]{0:T(128)S(1)}, f32[128]{0:T(128)}, u32[]{:S(2)}) copy-start(f32[128]{0:T(128)} %get-tuple-element.48) | copy-start | bytes 1540
  290.6 23.8 %copy-start.25 = (f32[128]{0:T(128)S(1)}, f32[128]{0:T(128)}, u32[]{:S(2)}) copy-start(f32[128]{0:T(128)} %get-tuple-element.49) | copy-start | bytes 1540
  290.7 23.8 %copy-start.26 = (f32[128]{0:T(128)S(1)}, f32[128]{0:T(128)}, u32[]{:S(2)}) copy-start(f32[128]{0:T(128)} %get-tuple-element.50) | copy-start | bytes 1540
  290.7 23.8 %copy-start.27 = (f32[128]{0:T(128)S(1)}, f32[128]{0:T(128)}, u32[]{:S(2)}) copy-start(f32[128]{0:T(128)} %get-tuple-element.51) | copy-start | bytes 1540
  290.7 23.8 %copy-start.28 = (f32[128]{0:T(128)S(1)}, f32[128]{0:T(128)}, u32[]{:S(2)}) copy-start(f32[128]{0:T(128)} %get-tuple-element.52) | copy-start | bytes 1540
  290.7 23.8 %copy-start.29 = (f32[128]{0:T(128)S(1)}, f32[128]{0:T(128)}, u32[]{:S(2)}) copy-start(f32[128]{0:T(128)} %get-tuple-element.53) | copy-start | bytes 1540
  290.7 23.8 %copy-start.30 = (f32[128]{0:T(128)S(1)}, f32[128]{0:T(128)}, u32[]{:S(2)}) copy-start(f32[128]{0:T(128)} %get-tuple-element.54) | copy-start | bytes 1540
  290.7 23.8 %copy-start.31 = (f32[128]{0:T(128)S(1)}, f32[128]{0:T(128)}, u32[]{:S(2)}) copy-start(f32[128]{0:T(128)} %get-tuple-element.55) | copy-start | bytes 1540
  290.7 23.8 %copy-start.32 = (f32[128]{0:T(128)S(1)}, f32[128]{0:T(128)}, u32[]{:S(2)}) copy-start(f32[128]{0:T(128)} %get-tuple-element.56) | copy-start | bytes 1540
  290.7 23.8 %copy-start.33 = (f32[128]{0:T(128)S(1)}, f32[128]{0:T(128)}, u32[]{:S(2)}) copy-start(f32[128]{0:T(128)} %get-tuple-element.57) | copy-start | bytes 1540
  290.7 23.8 %copy-start.34 = (f32[128]{0:T(128)S(1)}, f32[128]{0:T(128)}, u32[]{:S(2)}) copy-start(f32[128]{0:T(128)} %get-tuple-element.58) | copy-start | bytes 1540
  294.5 21.9 %all-to-all-start.4 = ((bf16[16,256,128]{2,1,0:T(8,128)(2,1)}), bf16[16,256,128]{2,1,0:T(8,128)(2,1)S(1)}, u32[]{:S(2)}, u32[]{:S(2)}) async-start(bf16[16,256,128]{2,1,0:T(8,128)(2,1)} %bitcast.17), calls=%async_computation.5 | async-start | bytes 2097152 | tf_op jit(solution)/shard_map/all_to_all | solution.py:58
  301.4 12.9 %collective-permute-start = (f32[30,128]{1,0:T(8,128)S(1)}, f32[30,128]{1,0:T(8,128)S(1)}, u32[]{:S(2)}, u32[]{:S(2)}) collective-permute-start(f32[30,128]{1,0:T(8,128)S(1)} %slice.309), channel_id=1, source_target_pairs={{16,0},{32,16},{48,32},{64,48},{80,64},{96,80},{112,96},{128,112},... | collective-permute-start | bytes 46088 | tf_op jit(solution)/shard_map/ppermute | solution.py:65
Sparse Core Ops, SparseCore 0:
  51.8 82.0 all-gather.2
  152.1 61.6 reduce-scatter.1
  245.3 34.2 all-gather.4
where the time goes:
time: 327 us; the launch traced here: 324 us
  waiting for transfers between devices  179 us (55%)
  matrix products  41.4 us (13%)
  starting transfers between devices  34.6 us (11%)
  blocking collectives  30.9 us (9%)
  between operations  14.4 us (4%)
  local copies, waits for them, and re-layouts  14 us (4%)
  other arithmetic  9.31 us (3%)
    all_gather x1, waiting for transfers between devices, in_one_piece(): out = lax.all_gather(both, axis, axis=dim, tiled=True)  82 us
    reduce_scatter x1, waiting for transfers between devices, per_device(): lax.psum_scatter(input_part.astype(jnp.bfloat16), 'tp', scatter_dimension...  61.8 us
    all_to_all x3, starting transfers between devices, sent_to_all(): lax.all_to_all(jnp.broadcast_to(value[None], (count, *value.shape)), axis...  23.1 us
    all_gather x1, waiting for transfers between devices, per_device(): full_grad = lax.all_gather(stream_grad, 'tp', axis=1, tiled=True)  21.2 us
    all_to_all x1, blocking collectives, side_by_side(): lax.all_to_all(both, axis, split_axis=split_dim, concat_axis=concat_dim,...  18.3 us
    all_to_all x1, blocking collectives, per_device(): lax.all_to_all(input_back.reshape(token_groups, capacity, width_part), 's...  12.6 us
    all_to_all x3, waiting for transfers between devices, sent_to_all(): lax.all_to_all(jnp.broadcast_to(value[None], (count, *value.shape)), axis...  10.7 us
    all_to_all x1, starting transfers between devices, sent_and_summed(): lax.all_to_all(cut_along(value, dim, count), axis, 0, 0, tiled=True)  6.68 us
  transfers between devices with their start and end apart: 8, of which 6 were waited for; matrix products, arithmetic and copies ran while one was open for 10% of the time, Pallas kernels for 0%

commit v1 on v0

v1 whole, which is shorter than its diff:
```python
import jax
import jax.numpy as jnp
from jax import lax
from jax.experimental import pallas as pl
from jax.experimental.pallas import tpu as pltpu
from jax.sharding import PartitionSpec as P

MESH = pl.DeviceIdType.MESH
F32, BF16 = jnp.float32, jnp.bfloat16
EPSILON = 1e-06
NZ, NS = 8, 16
TOK, W, CH = 256, 256, 128
CAP, ROWS, HALF = 48, 768, 384
MODEL, CHANNELS, TAPS = 4096, 2048, 31
STEPS = ((0, 0), (0, 1), (1, 0), (1, 1))
OFFSETS = (0, 1, -1, 2, -2, 3, -3, 4)


def dot(a, b, ca, cb):
    return lax.dot_general(a, b, (((ca,), (cb,)), ((), ())), preferred_element_type=F32)


def columns_to_rows(columns):
    lane = lax.broadcasted_iota(jnp.int32, (TOK, 128), 1)
    packed = jnp.zeros((TOK, 128), F32)
    for k, column in enumerate(columns):
        packed = jnp.where(lane == k, column, packed)
    return packed.T[0:8, :]


def rows_to_columns(rows):
    return jnp.concatenate([rows, jnp.zeros((120, TOK), F32)], axis=0).T


def silu_slope(values, logistic):
    return logistic * (1.0 + values * (1.0 - logistic))


def comm_kernel(
    gain_ref, routes_ref, rw_ref, lng_ref, up_h, st_h, wg_h, wu_h, wd_h, cp_h, wo_h,
    gg_h, gu_h, gd_h, cb_o, go_o,
    UP, ST, CP, WC, WD, WO, PICK, SW, SI, SC, X, CT, G, A, CAT, ACT, GG, GU, GD,
    SB, SR, RSS, RSR, FIN, RET, SG, MB, MO, CEN, SCL, HS, HALO, GOS, GOR, SS, SX,
    ls, ups, upr, xs, xr, dxs, dxr, as_, ar, cs, cr, dcs, dcr, sbs, sbr, rss, rsr,
    es, er, fs, fr, sgs, sgr, dgs, dgr, gs, gr, hs, hr,
):
    sp = lax.axis_index("sp")
    tp = lax.axis_index("tp")
    z = tp // 2
    c = tp % 2
    sibling = (sp, z * 2 + 1 - c)

    def zat(offset):
        return (z + offset + NZ) % NZ

    def zdev(offset):
        return (sp, zat(offset) * 2 + c)

    def mine(offset):
        return zat(offset) * 2 + c

    def other(offset):
        return zat(offset) * 2 + 1 - c

    def remote(src, dst, ssem, rsem, device):
        return pltpu.make_async_remote_copy(
            src_ref=src, dst_ref=dst, send_sem=ssem, recv_sem=rsem,
            device_id=device, device_id_type=MESH,
        )

    def each_peer(body):
        def step(k, carry):
            body((sp + k) % NS)
            return carry

        lax.fori_loop(1, NS, step, 0)

    barrier = pltpu.get_barrier_semaphore()

    def greet(k, carry):
        pl.semaphore_signal(barrier, inc=1, device_id=(sp, (tp + k) % NS), device_id_type=MESH)
        pl.semaphore_signal(barrier, inc=1, device_id=((sp + k) % NS, tp), device_id_type=MESH)
        return carry

    lax.fori_loop(1, NS, greet, 0)
    loads = [
        pltpu.make_async_copy(up_h, UP.at[z], ls.at[0]),
        pltpu.make_async_copy(st_h, ST, ls.at[1]),
        pltpu.make_async_copy(cp_h, CP, ls.at[2]),
        pltpu.make_async_copy(wg_h, WC.at[:, pl.ds(0, CH)], ls.at[3]),
        pltpu.make_async_copy(wu_h, WC.at[:, pl.ds(CH, CH)], ls.at[4]),
        pltpu.make_async_copy(wd_h, WD, ls.at[5]),
        pltpu.make_async_copy(wo_h, WO, ls.at[6]),
    ]
    for load in loads:
        load.start()
    pl.semaphore_wait(barrier, 2 * (NS - 1))

    def active(t, d, h):
        return t <= 3 or d == h

    def ring(buf, index, half, ssem, rsem, t, d, h, arriving):
        sign = 1 - 2 * d
        block = buf.at[index(-sign * (t if arriving else t - 1)), pl.ds(h * half, half)]
        return remote(block, block, ssem.at[d, t - 1, h], rsem.at[d, t - 1, h], zdev(sign))

    def ring_send(*args):
        ring(*args, False).start()

    def ring_take(*args):
        ring(*args, True).wait_recv()

    def up_send(t):
        for d, h in STEPS:
            if active(t, d, h):
                ring_send(UP, zat, TOK // 2, ups, upr, t, d, h)

    def up_take(t):
        for d, h in STEPS:
            if active(t, d, h):
                ring_take(UP, zat, TOK // 2, ups, upr, t, d, h)

    loads[0].wait()
    up_send(1)

    def exchange_start(n, rows):
        SX[n] = rows
        SS[n, tp] = rows

        def step(k, carry):
            peer = (tp + k) % NS
            remote(SX.at[n], SS.at[n, tp], es.at[n], er.at[n], (sp, peer)).start()
            return carry

        lax.fori_loop(1, NS, step, 0)

    def exchange_end(n):
        many = SS.at[n, pl.ds(0, NS - 1)]
        remote(many, many, es.at[n], er.at[n], sibling).wait_recv()
        return rows_to_columns(jnp.sum(SS[n], axis=0))

    def exchange_flush(n):
        many = SS.at[n, pl.ds(0, NS - 1)]
        remote(many, many, es.at[n], er.at[n], sibling).wait_send()

    loads[1].wait()
    loads[2].wait()
    stream = ST[...].astype(F32)
    conv = CP[...].astype(F32)
    exchange_start(
        0,
        columns_to_rows([
            jnp.sum(stream * stream, axis=1, keepdims=True),
            jnp.sum(conv, axis=1, keepdims=True),
            jnp.sum(conv * conv, axis=1, keepdims=True),
        ]),
    )

    first, second = routes_ref[0:1, :], routes_ref[1:2, :]
    names = lax.broadcasted_iota(jnp.int32, (NS, TOK), 0)
    hit0 = (names == first).astype(F32)
    hit1 = (names == second).astype(F32)
    earlier = (
        lax.broadcasted_iota(jnp.int32, (TOK, TOK), 0) < lax.broadcasted_iota(jnp.int32, (TOK, TOK), 1)
    ).astype(F32).astype(BF16)
    rank = dot((hit0 + hit1).astype(BF16), earlier, 1, 0)
    slot0 = first * CAP + jnp.sum(hit0 * rank, axis=0, keepdims=True).astype(jnp.int32)
    slot1 = second * CAP + jnp.sum(hit1 * rank, axis=0, keepdims=True).astype(jnp.int32)
    for r in range(3):
        slots = lax.broadcasted_iota(jnp.int32, (TOK, TOK), 0) + r * TOK
        at0, at1 = slots == slot0, slots == slot1
        rows = pl.ds(r * TOK, TOK)
        PICK[rows, :] = jnp.logical_or(at0, at1).astype(F32).astype(BF16)
        SW[rows, :] = jnp.sum(
            jnp.where(at0, rw_ref[0:1, :], 0.0) + jnp.where(at1, rw_ref[1:2, :], 0.0),
            axis=1, keepdims=True,
        )

    def slot_rows(p):
        return pl.ds(pl.multiple_of(p * CAP, 16), CAP)

    def send_cotangent(offset):
        origin = zat(offset)
        block = mine(offset)

        def pick(r, carry):
            rows = pl.ds(pl.multiple_of(r * TOK, TOK), TOK)
            SC[origin, rows, :] = (dot(PICK[rows, :], UP[origin], 1, 0) * SW[rows, :]).astype(BF16)
            return carry

        lax.fori_loop(0, 3, pick, 0)

        def send(p):
            remote(
                SC.at[origin, slot_rows(p)], CT.at[block, slot_rows(sp)],
                cs.at[origin], cr.at[origin], (p, tp),
            ).start()

        each_peer(send)
        CT[block, slot_rows(sp), :] = SC[origin, slot_rows(sp), :]

    send_cotangent(0)
    up_take(1)
    up_send(2)

    stats = exchange_end(0)
    inverse = lax.rsqrt(stats[:, 0:1] / MODEL + EPSILON)
    mean_val = stats[:, 1:2] / CHANNELS
    inv_std = lax.rsqrt(stats[:, 2:3] / CHANNELS - mean_val * mean_val + EPSILON)
    normed = (gain_ref[...] * ST[...].astype(F32) * inverse).astype(BF16)
    for r in range(3):
        rows = pl.ds(r * TOK, TOK)
        SI[rows, :] = dot(PICK[rows, :], normed, 1, 0).astype(BF16)
    own = mine(0)

    def send_input(p):
        remote(SI.at[slot_rows(p)], X.at[own, slot_rows(sp)], as_.at[0], ar.at[0], (p, tp)).start()

    each_peer(send_input)
    X[own, slot_rows(sp), :] = SI[slot_rows(sp), :]

    send_cotangent(1)
    send_cotangent(-1)
    up_take(2)
    up_send(3)
    send_cotangent(2)
    send_cotangent(-2)
    up_take(3)
    up_send(4)
    send_cotangent(3)
    send_cotangent(-3)

    centred = (CP[...].astype(F32) - mean_val) * inv_std
    scaled = centred * lng_ref[...]
    CEN[...] = centred
    SCL[...] = scaled
    MO[...] = (scaled * jax.nn.sigmoid(scaled)).astype(BF16)
    G[...] = jnp.zeros_like(G)
    A[...] = jnp.zeros_like(A)

    up_take(4)
    send_cotangent(4)
    for k in range(3, 6):
        loads[k].wait()

    def take_many(dst, ssem, rsem):
        remote(dst, dst, ssem, rsem, sibling).wait_recv()

    def flush_many(src, ssem, rsem):
        remote(src, src, ssem, rsem, sibling).wait_send()

    def cols(j):
        return pl.ds(pl.multiple_of(j * W, W), W)

    def add_inputs(j):
        def step(r, carry):
            rows = pl.ds(pl.multiple_of(r * TOK, TOK), TOK)
            G[rows, :] = G[rows, :] + dot(X[j, rows, :], WC[cols(j), :], 1, 0)
            return carry

        lax.fori_loop(0, 3, step, 0)

    def add_cotangents(j):
        def step(r, carry):
            rows = pl.ds(pl.multiple_of(r * TOK, TOK), TOK)
            A[rows, :] = A[rows, :] + dot(CT[j, rows, :], WD[:, cols(j)], 1, 1)
            return carry

        lax.fori_loop(0, 3, step, 0)

    def hand_over(t, d, h, offset, arriving):
        j = other(offset) if arriving else mine(offset)
        block = X.at[j, pl.ds(h * HALF, HALF)]
        return remote(block, block, dxs.at[t, d, h], dxr.at[t, d, h], sibling)

    def x_ring(t, d, h):
        return (X, mine, HALF, xs, xr, t, d, h)

    def hand_cotangent(offset, arriving):
        j = other(offset) if arriving else mine(offset)
        return remote(CT.at[j], CT.at[j], dcs.at[zat(offset)], dcr.at[zat(offset)], sibling)

    take_many(X.at[own, pl.ds(0, ROWS - CAP)], as_.at[0], ar.at[0])
    for d, h in STEPS:
        ring_send(*x_ring(1, d, h))
    for h in range(2):
        hand_over(0, 0, h, 0, False).start()
    add_inputs(own)

    def stage_offsets(t):
        return (0,) if t == 0 else ((t, -t) if t < 4 else (4,))

    def x_chunks(t):
        if t == 0:
            return [(0, 0, 0), (0, 1, 0)]
        return [(d, h, -t * (1 - 2 * d)) for h in range(2) for d in range(2) if active(t, d, h)]

    def from_sibling(t):
        for d, h, offset in x_chunks(t):
            hand_over(t, d, h, offset, True).wait_recv()
        for offset in stage_offsets(t):
            add_inputs(other(offset))

    def cot_from_sibling(t):
        for offset in OFFSETS[2 * t - 2 : 2 * t]:
            hand_cotangent(offset, True).wait_recv()
            add_cotangents(other(offset))

    for t in range(1, 5):
        for d, h, offset in x_chunks(t):
            ring_take(*x_ring(t, d, h))
            if t < 4 and active(t + 1, d, h):
                ring_send(*x_ring(t + 1, d, h))
            hand_over(t, d, h, offset, False).start()
        for offset in stage_offsets(t):
            add_inputs(mine(offset))
        from_sibling(t - 1)
        for offset in OFFSETS[2 * t - 2 : 2 * t]:
            take_many(CT.at[mine(offset), pl.ds(0, ROWS - CAP)], cs.at[zat(offset)], cr.at[zat(offset)])
            hand_cotangent(offset, False).start()
            add_cotangents(mine(offset))
        if t > 1:
            cot_from_sibling(t - 1)
    from_sibling(4)
    cot_from_sibling(4)

    def hidden(r, carry):
        rows = pl.ds(pl.multiple_of(r * 64, 64), 64)
        gate, upper, back = G[rows, 0:CH], G[rows, CH : 2 * CH], A[rows, :]
        logistic = jax.nn.sigmoid(gate)
        silu = gate * logistic
        ACT[rows, :] = (silu * upper).astype(BF16)
        CAT[rows, 0:CH] = (back * upper * silu_slope(gate, logistic)).astype(BF16)
        CAT[rows, CH : 2 * CH] = (back * silu).astype(BF16)
        return carry

    lax.fori_loop(0, 12, hidden, 0)

    def sub_rows(h, r):
        return pl.ds(pl.multiple_of(h * HALF + r * 128, 128), 128)

    def for_sibling(offset):
        q = zat(offset)
        j = other(offset)

        def step(r, carry):
            rows = pl.ds(pl.multiple_of(r * TOK, TOK), TOK)
            SB[q, rows, :] = dot(CAT[rows, :], WC[cols(j), :], 1, 1).astype(BF16)
            return carry

        lax.fori_loop(0, 3, step, 0)
        remote(SB.at[q], SR.at[q], sbs.at[q], sbr.at[q], sibling).start()

    def take_sibling(offset):
        q = zat(offset)
        remote(SB.at[q], SR.at[q], sbs.at[q], sbr.at[q], sibling).wait_recv()

    def chip_part(offset, rows):
        return dot(CAT[rows, :], WC[cols(mine(offset)), :], 1, 1) + SR[zat(offset), rows, :].astype(F32)

    def rs_copy(d, k, h):
        part = pl.ds(h * HALF, HALF)
        return remote(
            RSS.at[d, k, part], RSR.at[d, k, part], rss.at[d, k, h], rsr.at[d, k, h], zdev(1 - 2 * d)
        )

    def rs_active(k, d, h):
        return k >= 1 or d == h

    def rs_send(k, d, h):
        offset = (4 - k) * (1 - 2 * d)
        incoming = k >= 1 and rs_active(k - 1, d, h)
        if incoming:
            rs_copy(d, k - 1, h).wait_recv()

        def step(r, carry):
            rows = sub_rows(h, r)
            total = chip_part(offset, rows)
            if incoming:
                total = total + RSR[d, k - 1, rows, :].astype(F32)
            RSS[d, k, rows, :] = total.astype(BF16)
            return carry

        lax.fori_loop(0, 3, step, 0)
        rs_copy(d, k, h).start()

    def gradients(first_block):
        def step(b, carry):
            j = first_block + b
            both = dot(X[j], CAT[...], 0, 0)
            GG[cols(j), :] = both[:, 0:CH]
            GU[cols(j), :] = both[:, CH : 2 * CH]
            GD[:, cols(j)] = dot(ACT[...], CT[j], 0, 0)
            return carry

        lax.fori_loop(0, 4, step, 0)

    for_sibling(4)
    for_sibling(3)
    for_sibling(-3)
    take_sibling(4)
    rs_send(0, 0, 0)
    rs_send(0, 1, 1)
    for_sibling(2)
    for_sibling(-2)
    take_sibling(3)
    take_sibling(-3)
    rs_send(1, 0, 1)
    rs_send(1, 1, 0)
    for_sibling(1)
    for_sibling(-1)
    for_sibling(0)
    rs_send(1, 0, 0)
    rs_send(1, 1, 1)
    gradients(0)
    take_sibling(2)
    take_sibling(-2)
    rs_send(2, 0, 1)
    rs_send(2, 1, 0)
    rs_send(2, 0, 0)
    rs_send(2, 1, 1)
    gradients(4)
    gradients(8)
    take_sibling(1)
    take_sibling(-1)
    rs_send(3, 0, 1)
    rs_send(3, 1, 0)
    rs_send(3, 0, 0)
    rs_send(3, 1, 1)
    gradients(12)
    stores = [
        pltpu.make_async_copy(GG, gg_h, ls.at[7]),
        pltpu.make_async_copy(GU, gu_h, ls.at[8]),
        pltpu.make_async_copy(GD, gd_h, ls.at[9]),
    ]
    for store in stores:
        store.start()
    take_sibling(0)
    for h in (1, 0):
        rs_copy(0, 3, h).wait_recv()
        rs_copy(1, 3, h).wait_recv()

        def finish(r, carry):
            rows = sub_rows(h, r)
            FIN[rows, :] = (
                chip_part(0, rows) + RSR[0, 3, rows, :].astype(F32) + RSR[1, 3, rows, :].astype(F32)
            ).astype(BF16)
            return carry

        lax.fori_loop(0, 3, finish, 0)

    def send_back(p):
        remote(FIN.at[slot_rows(p)], RET.at[slot_rows(sp)], fs.at[0], fr.at[0], (p, tp)).start()

    each_peer(send_back)
    RET[slot_rows(sp), :] = FIN[slot_rows(sp), :]
    take_many(RET.at[pl.ds(0, ROWS - CAP)], fs.at[0], fr.at[0])

    gained = gain_ref[...] * dot(PICK[...], RET[...], 0, 0)
    residual = ST[...].astype(F32)
    exchange_start(1, columns_to_rows([jnp.sum(gained * residual, axis=1, keepdims=True)]))
    inner = exchange_end(1)[:, 0:1] / MODEL
    SG[own] = (
        UP[z].astype(F32) + inverse * gained - residual * (inverse * inverse * inverse * inner)
    ).astype(BF16)

    def sg_ring(t, d, h):
        return (SG, mine, TOK // 2, sgs, sgr, t, d, h)

    def sg_hand(t, d, h, offset, arriving):
        j = other(offset) if arriving else mine(offset)
        block = SG.at[j, pl.ds(h * (TOK // 2), TOK // 2)]
        return remote(block, block, dgs.at[t, d, h], dgr.at[t, d, h], sibling)

    for d, h in STEPS:
        ring_send(*sg_ring(1, d, h))
    for h in range(2):
        sg_hand(0, 0, h, 0, False).start()
    loads[6].wait()

    def mix(j):
        MB[...] = MB[...] + dot(SG[j], WO[:, cols(j)], 1, 1)

    MB[...] = jnp.zeros_like(MB)
    mix(own)
    for t in range(1, 5):
        for d, h, offset in x_chunks(t):
            ring_take(*sg_ring(t, d, h))
            if t < 4 and active(t + 1, d, h):
                ring_send(*sg_ring(t + 1, d, h))
            sg_hand(t, d, h, offset, False).start()
        for offset in stage_offsets(t):
            mix(mine(offset))
        for d, h, offset in x_chunks(t - 1):
            sg_hand(t - 1, d, h, offset, True).wait_recv()
        for offset in stage_offsets(t - 1):
            mix(other(offset))
    for d, h, offset in x_chunks(4):
        sg_hand(4, d, h, offset, True).wait_recv()
    mix(other(4))

    scaled = SCL[...]
    norm_in = MB[...] * silu_slope(scaled, jax.nn.sigmoid(scaled)) * lng_ref[...]
    exchange_start(
        2,
        columns_to_rows([
            jnp.sum(norm_in, axis=1, keepdims=True),
            jnp.sum(norm_in * CEN[...], axis=1, keepdims=True),
        ]),
    )

    def out_block(p):
        GOS[p] = dot(MO[...], SG[p], 0, 0).astype(BF16)
        remote(GOS.at[p], GOR.at[sp], gs.at[0], gr.at[0], (p, tp)).start()

    def out_blocks(low, high):
        def step(k, carry):
            out_block((sp + k) % NS)
            return carry

        lax.fori_loop(low, high, step, 0)

    out_blocks(1, 6)
    sums = exchange_end(2)
    conv_back = inv_std * (
        norm_in - sums[:, 0:1] / CHANNELS - CEN[...] * (sums[:, 1:2] / CHANNELS)
    )
    HS[...] = conv_back[0:32, :]
    previous = ((sp + NS - 1) % NS, tp)

    @pl.when(sp > 0)
    def _():
        remote(HS, HALO, hs.at[0], hr.at[0], previous).start()

    cb_o[0:TOK, :] = conv_back
    out_blocks(6, NS)
    GOR[sp] = dot(MO[...], SG[sp], 0, 0).astype(BF16)

    @pl.when(sp < NS - 1)
    def _():
        remote(HS, HALO, hs.at[0], hr.at[0], previous).wait_recv()
        cb_o[TOK : TOK + 32, :] = HALO[...]

    @pl.when(sp == NS - 1)
    def _():
        cb_o[TOK : TOK + 32, :] = jnp.zeros((32, CH), F32)

    take_many(GOR.at[pl.ds(0, NS - 1)], gs.at[0], gr.at[0])

    def total(i, acc):
        return acc + GOR[i].astype(F32)

    go_o[...] = lax.fori_loop(0, NS, total, jnp.zeros((CH, W), F32))

    for t in range(1, 5):
        for d, h in STEPS:
            if active(t, d, h):
                ring(UP, zat, TOK // 2, ups, upr, t, d, h, False).wait_send()
                ring(*x_ring(t, d, h), False).wait_send()
                ring(*sg_ring(t, d, h), False).wait_send()
    for t in range(5):
        for d, h, offset in x_chunks(t):
            hand_over(t, d, h, offset, False).wait_send()
            sg_hand(t, d, h, offset, False).wait_send()
    for offset in OFFSETS:
        q = zat(offset)
        flush_many(SC.at[q, pl.ds(0, ROWS - CAP)], cs.at[q], cr.at[q])
        hand_cotangent(offset, False).wait_send()
        remote(SB.at[q], SR.at[q], sbs.at[q], sbr.at[q], sibling).wait_send()
    for k in range(4):
        for d, h in STEPS:
            if rs_active(k, d, h):
                rs_copy(d, k, h).wait_send()
    for n in range(3):
        exchange_flush(n)
    flush_many(SI.at[pl.ds(0, ROWS - CAP)], as_.at[0], ar.at[0])
    flush_many(FIN.at[pl.ds(0, ROWS - CAP)], fs.at[0], fr.at[0])
    flush_many(GOS.at[pl.ds(0, NS - 1)], gs.at[0], gr.at[0])

    @pl.when(sp > 0)
    def _():
        remote(HS, HALO, hs.at[0], hr.at[0], previous).wait_send()

    for store in stores:
        store.wait()


def last_kernel(
    gg_i, gu_i, gd_i, cb_ref, taps_ref, value_ref, gate_ref,
    gg_o, gu_o, gd_o, vg_o, tg_o, bufs_tall, buf_wide, lsem, ssem,
):
    pieces = []
    for a, (src, dst) in enumerate(((gg_i, gg_o), (gu_i, gu_o))):
        for q in range(4):
            part = pl.ds(q * 1024, 1024)
            pieces.append((src.at[part], bufs_tall.at[a, part], dst.at[part]))
    for q in range(4):
        part = pl.ds(q * 32, 32)
        pieces.append((gd_i.at[part], buf_wide.at[part], gd_o.at[part]))
    ins = [pltpu.make_async_copy(s, b, lsem.at[n]) for n, (s, b, _) in enumerate(pieces)]
    outs = [pltpu.make_async_copy(b, d, ssem.at[n]) for n, (_, b, d) in enumerate(pieces)]
    for copy in ins:
        copy.start()
    for i, o in zip(ins, outs):
        i.wait()
        o.start()
    acc = jnp.zeros((TOK, CH), F32)
    for tap in range(TAPS):
        acc = acc + taps_ref[tap : tap + 1, :] * cb_ref[TAPS - 1 - tap : TAPS - 1 - tap + TOK, :]
    sigma = jax.nn.sigmoid(gate_ref[...].astype(F32))
    vg_o[...] = (acc * sigma).astype(BF16)
    tg_o[...] = (acc * value_ref[...].astype(F32) * sigma * (1.0 - sigma)).astype(BF16)
    for copy in outs:
        copy.wait()


def shape(dims, dtype):
    return jax.ShapeDtypeStruct(dims, dtype)


def per_device(
    upstream, stream, norm_gain, routes, route_weights, w_gate, w_up, w_down,
    value_in, gate_in, conv_pre, ln_gain, conv_taps, w_out,
):
    near, far = pl.BlockSpec(memory_space=pltpu.VMEM), pl.BlockSpec(memory_space=pl.ANY)
    dma, vm = pltpu.SemaphoreType.DMA, pltpu.VMEM
    grads = [shape((MODEL, CH), F32), shape((MODEL, CH), F32), shape((CH, MODEL), F32)]
    scratch = [
        vm((NZ, TOK, W), BF16), vm((TOK, W), BF16), vm((TOK, CH), BF16),
        vm((MODEL, 2 * CH), BF16), vm((CH, MODEL), BF16), vm((CH, MODEL), BF16),
        vm((ROWS, TOK), BF16), vm((ROWS, 1), F32),
        vm((ROWS, W), BF16), vm((NZ, ROWS, W), BF16),
        vm((NS, ROWS, W), BF16), vm((NS, ROWS, W), BF16),
        vm((ROWS, 2 * CH), F32), vm((ROWS, CH), F32),
        vm((ROWS, 2 * CH), BF16), vm((ROWS, CH), BF16),
        vm((MODEL, CH), F32), vm((MODEL, CH), F32), vm((CH, MODEL), F32),
        vm((NZ, ROWS, W), BF16), vm((NZ, ROWS, W), BF16),
        vm((2, 4, ROWS, W), BF16), vm((2, 4, ROWS, W), BF16),
        vm((ROWS, W), BF16), vm((ROWS, W), BF16),
        vm((NS, TOK, W), BF16), vm((TOK, CH), F32),
        vm((TOK, CH), BF16), vm((TOK, CH), F32), vm((TOK, CH), F32),
        vm((32, CH), F32), vm((32, CH), F32),
        vm((NS, CH, W), BF16), vm((NS, CH, W), BF16),
        vm((3, NS, 8, TOK), F32), vm((3, 8, TOK), F32),
        dma((10,)),
        dma((2, 4, 2)), dma((2, 4, 2)), dma((2, 4, 2)), dma((2, 4, 2)),
        dma((5, 2, 2)), dma((5, 2, 2)),
        dma((1,)), dma((1,)),
        dma((NZ,)), dma((NZ,)), dma((NZ,)), dma((NZ,)),
        dma((NZ,)), dma((NZ,)),
        dma((2, 4, 2)), dma((2, 4, 2)),
        dma((3,)), dma((3,)),
        dma((1,)), dma((1,)),
        dma((2, 4, 2)), dma((2, 4, 2)), dma((5, 2, 2)), dma((5, 2, 2)),
        dma((1,)), dma((1,)), dma((1,)), dma((1,)),
    ]
    gg, gu, gd, conv_back, grad_out = pl.pallas_call(
        comm_kernel,
        name="exchange",
        out_shape=grads + [shape((TOK + 32, CH), F32), shape((CH, W), F32)],
        in_specs=[near] * 4 + [far] * 7,
        out_specs=[far] * 3 + [near] * 2,
        scratch_shapes=scratch,
        compiler_params=pltpu.CompilerParams(
            collective_id=0, has_side_effects=True, vmem_limit_bytes=67_000_000
        ),
    )(
        norm_gain.reshape(1, W), routes.T, route_weights.T, ln_gain.reshape(1, CH),
        upstream, stream, w_gate[0], w_up[0], w_down[0], conv_pre, w_out,
    )
    grad_gate, grad_up, grad_down, value_grad, gate_grad = pl.pallas_call(
        last_kernel,
        name="last",
        out_shape=grads + [shape((TOK, CH), BF16)] * 2,
        in_specs=[far] * 3 + [near] * 4,
        out_specs=[far] * 3 + [near] * 2,
        scratch_shapes=[
            vm((2, MODEL, CH), F32), vm((CH, MODEL), F32), dma((12,)), dma((12,)),
        ],
        compiler_params=pltpu.CompilerParams(vmem_limit_bytes=40_000_000),
    )(gg, gu, gd, conv_back, conv_taps, value_in, gate_in)
    return (grad_gate[None], grad_up[None], grad_down[None], grad_out, value_grad, gate_grad)


def solution(mesh):
    return jax.shard_map(
        per_device,
        mesh=mesh,
        in_specs=(
            P("sp", "tp"), P("sp", "tp"), P("tp"), P("sp", None), P("sp", None),
            P("sp", None, "tp"), P("sp", None, "tp"), P("sp", "tp", None),
            P("sp", "tp"), P("sp", "tp"), P("sp", "tp"), P("tp"), P(None, "tp"), P("tp", None),
        ),
        out_specs=(
            P("sp", None, "tp"), P("sp", None, "tp"), P("sp", "tp", None),
            P("tp", "sp"), P("sp", "tp"), P("sp", "tp"),
        ),
        check_vma=False,
    )
```

time: 327 us -> 175 us (0.54)
  waiting for transfers between devices: 179 us -> 0 us
  Pallas kernels: 0 us -> 164 us
  matrix products: 41.4 us -> 0 us
  starting transfers between devices: 34.6 us -> 0 us
  blocking collectives: 30.9 us -> 0 us
  between operations: 14.4 us -> 0.69 us
  other arithmetic: 9.31 us -> 0 us
  local copies, waits for them, and re-layouts: 14 us -> 8.02 us
    pallas_call x0 -> x2, Pallas kernels: none -> 164 us  [the longest x1 160 us: per_device(): pl.pallas_call(comm_kernel, name='exchange', out_shape=grads + [shape((TO...]
    all_gather x2 -> x0, waiting for transfers between devices: 103 us -> none  [the longest x1 82 us: in_one_piece(): out = lax.all_gather(both, axis, axis=dim, tiled=True)]
    reduce_scatter x1 -> x0, waiting for transfers between devices: 61.8 us -> none  [per_device(): lax.psum_scatter(input_part.astype(jnp.bfloat16), 'tp', scatter_dimension...]
    dot_general x11 -> x0, matrix products: 41.4 us -> none  [the longest x1 6.03 us: per_device(): lax.dot_general(inputs, upper_back, (((0,), (0,)), ((), ())), preferred_e...]
    all_to_all x2 -> x0, blocking collectives: 30.9 us -> none  [the longest x1 18.3 us: side_by_side(): lax.all_to_all(both, axis, split_axis=split_dim, concat_axis=concat_dim,...]
    all_to_all x4 -> x0, starting transfers between devices: 29.8 us -> none  [the longest x3 23.1 us: sent_to_all(): lax.all_to_all(jnp.broadcast_to(value[None], (count, *value.shape)), axis...]
    all_to_all x4 -> x0, waiting for transfers between devices: 10.7 us -> none  [the longest x3 10.7 us: sent_to_all(): lax.all_to_all(jnp.broadcast_to(value[None], (count, *value.shape)), axis...]
    gather x2 -> x0, local copies, waits for them, and re-layouts: 5.31 us -> none  [the longest x1 2.66 us: per_device(): upstream_pad[slot_token].astype(jnp.float32) * slot_weight[:, None]]
  transfers between devices with their start and end apart: 8 -> 0, of which waited for: 6 -> 0; matrix products, arithmetic and copies ran while one was open for 10% -> 0% of each run, Pallas kernels for 0% -> 0%
where the time goes in v1:
time: 175 us; the launch traced here: 173 us
  Pallas kernels  164 us (94%)
  local copies, waits for them, and re-layouts  8.02 us (5%)
    pallas_call x1, Pallas kernels, per_device(): pl.pallas_call(comm_kernel, name='exchange', out_shape=grads + [shape((TO...  160 us
    unnamed x17, local copies, waits for them, and re-layouts  8.02 us
    pallas_call x1, Pallas kernels, per_device(): pl.pallas_call(last_kernel, name='last', out_shape=grads + [shape((TOK, C...  3.93 us

profile of v1, /device:TPU:17, one launch (start us, length us, event | category | flops | bytes accessed | tf_op | source)
XLA Modules:
  0.0 172.8 jit_solution(17042862106966510221)
XLA Ops:
  0.6 0.0 copy-start.6
  0.6 160.1 %exchange.1 = (f32[4096,128]{1,0:T(8,128)}, f32[4096,128]{1,0:T(8,128)}, f32[128,4096]{1,0:T(8,128)}, f32[288,128]{1,0:T(8,128)}, f32[128,256]{1,0:T(8,128)}) custom-call(f32[1,256]{1,0:T(1,128)} %bitcast.15, s32[2,256]{1,0:T(2,128)} %bitcast.13, f32[2,256]{1,0:T(2,128)} %bitcast.14, f32[1,128]{1,0:T(1,128)} %bitcast.16, bf16[256,256]{1,0:T(8,128)(2,1)} %up_h.1, ...), custom_call_target="tpu_custom_call" | custom-call | tf_op jit(solution)/shard_map/exchange/pallas_call | solution.py:657
  160.8 0.0 copy-done.6
  160.8 0.0 copy-start
  160.8 1.6 copy-done
  162.4 0.0 copy-start.1
  162.4 1.6 copy-done.1
  164.0 0.0 copy-start.2
  164.0 1.6 copy-done.2
  165.6 0.0 copy-start.3
  165.6 0.9 copy-done.3
  166.5 0.0 copy-start.4
  166.5 0.8 copy-done.4
  167.3 0.0 copy-start.5
  167.3 0.8 copy-done.5
  168.2 0.0 copy-start.7
  168.2 3.9 %last.1 = (f32[4096,128]{1,0:T(8,128)}, f32[4096,128]{1,0:T(8,128)}, f32[128,4096]{1,0:T(8,128)}, bf16[256,128]{1,0:T(8,128)(2,1)}, bf16[256,128]{1,0:T(8,128)(2,1)}) custom-call(f32[4096,128]{1,0:T(8,128)S(1)} %copy-done, f32[4096,128]{1,0:T(8,128)S(1)} %copy-done.1, f32[128,4096]{1,0:T(8,128)S(1)} %copy-done.2, f32[288,128]{1,0:T(8,128)S(1)} %copy-done.3, ...), custom_call_target="tpu_custom_call" | custom-call | tf_op jit(solution)/shard_map/last/pallas_call | solution.py:671
  172.1 0.0 copy-done.7
  172.1 0.7 copy.21
Async XLA Ops:
  0.6 160.2 %copy-start.6 = (f32[31,128]{1,0:T(8,128)S(1)}, f32[31,128]{1,0:T(8,128)}, u32[]{:S(2)}) copy-start(f32[31,128]{1,0:T(8,128)} %taps_ref.1) | copy-start | bytes 47620
  160.8 1.6 copy-start
  162.4 1.6 copy-start.1
  164.0 1.6 copy-start.2
  165.6 0.9 copy-start.3
  166.5 0.8 copy-start.4
  167.3 0.8 copy-start.5
  168.2 3.9 %copy-start.7 = (f32[128,256]{1,0:T(8,128)S(1)}, f32[128,256]{1,0:T(8,128)}, u32[]{:S(2)}) copy-start(f32[128,256]{1,0:T(8,128)} %get-tuple-element.35) | copy-start | bytes 393220

commit v2 on v1

--- a/solution.py
+++ b/solution.py
@@ -39,10 +39,10 @@
 def comm_kernel(
     gain_ref, routes_ref, rw_ref, lng_ref, up_h, st_h, wg_h, wu_h, wd_h, cp_h, wo_h,
     gg_h, gu_h, gd_h, cb_o, go_o,
-    UP, ST, CP, WC, WD, WO, PICK, SW, SI, SC, X, CT, G, A, CAT, ACT, GG, GU, GD,
-    SB, SR, RSS, RSR, FIN, RET, SG, MB, MO, CEN, SCL, HS, HALO, GOS, GOR, SS, SX,
-    ls, ups, upr, xs, xr, dxs, dxr, as_, ar, cs, cr, dcs, dcr, sbs, sbr, rss, rsr,
-    es, er, fs, fr, sgs, sgr, dgs, dgr, gs, gr, hs, hr,
+    UP, XS, CP, WC, WD, WO, PICK, SW, SI, SC, X, CT, G, A, CAT, ACT, GG, GU, GD,
+    SB, SR, RSS, RSR, PB, RB, TSS, TSR, TB, AP, FIN, RET, SG, MB, MO, CEN, SCL, HS, HALO, GOS, GOR, SS, SX,
+    ls, ups, upr, xs, xr, dxs, dxr, as_, ar, cs, cr, dcs, dcr, sbs, sbr, rss, rsr, bs, br, tss, tsr,
+    sts, str_, dts, dtr, es, er, fs, fr, sgs, sgr, dgs, dgr, gs, gr, hs, hr,
 ):
     sp = lax.axis_index("sp")
     tp = lax.axis_index("tp")
@@ -85,7 +85,7 @@
     lax.fori_loop(1, NS, greet, 0)
     loads = [
         pltpu.make_async_copy(up_h, UP.at[z], ls.at[0]),
-        pltpu.make_async_copy(st_h, ST, ls.at[1]),
+        pltpu.make_async_copy(st_h, XS.at[mine(0)], ls.at[1]),
         pltpu.make_async_copy(cp_h, CP, ls.at[2]),
         pltpu.make_async_copy(wg_h, WC.at[:, pl.ds(0, CH)], ls.at[3]),
         pltpu.make_async_copy(wu_h, WC.at[:, pl.ds(CH, CH)], ls.at[4]),
@@ -94,7 +94,6 @@
     ]
     for load in loads:
         load.start()
-    pl.semaphore_wait(barrier, 2 * (NS - 1))
 
     def active(t, d, h):
         return t <= 3 or d == h
@@ -110,23 +109,50 @@
     def ring_take(*args):
         ring(*args, True).wait_recv()
 
-    def up_send(t):
-        for d, h in STEPS:
-            if active(t, d, h):
-                ring_send(UP, zat, TOK // 2, ups, upr, t, d, h)
+    def halves_ring(buf, ssem, rsem):
+        def send(t):
+            for h in range(2):
+                for d in range(2):
+                    if active(t, d, h):
+                        ring_send(buf, mine, TOK // 2, ssem, rsem, t, d, h)
+
+        def hand(t, d, h, offset, arriving, hs_, hr_):
+            j = other(offset) if arriving else mine(offset)
+            block = buf.at[j, pl.ds(h * (TOK // 2), TOK // 2)]
+            return remote(block, block, hs_.at[t, d, h], hr_.at[t, d, h], sibling)
+
+        return send, hand
+
+    def x_chunks(t):
+        if t == 0:
+            return [(0, 0, 0), (0, 1, 0)]
+        return [(d, h, -t * (1 - 2 * d)) for h in range(2) for d in range(2) if active(t, d, h)]
+
+    xs_send, xs_hand_ = halves_ring(XS, sts, str_)
+
+    def xs_hand(t, d, h, offset, arriving):
+        return xs_hand_(t, d, h, offset, arriving, dts, dtr)
+
+    def xs_take(t):
+        for d, h, offset in x_chunks(t):
+            ring_take(XS, mine, TOK // 2, sts, str_, t, d, h)
+            if t < 4 and active(t + 1, d, h):
+                ring_send(XS, mine, TOK // 2, sts, str_, t + 1, d, h)
+            xs_hand(t, d, h, offset, False).start()
 
     def up_take(t):
-        for d, h in STEPS:
-            if active(t, d, h):
-                ring_take(UP, zat, TOK // 2, ups, upr, t, d, h)
-
-    loads[0].wait()
-    up_send(1)
-
-    def exchange_start(n, rows):
+        for h in range(2):
+            for d in range(2):
+                if active(t, d, h):
+                    ring_take(UP, zat, TOK // 2, ups, upr, t, d, h)
+                    if t < 4 and active(t + 1, d, h):
+                        ring_send(UP, zat, TOK // 2, ups, upr, t + 1, d, h)
+
+    def exchange_set(n, rows):
         SX[n] = rows
         SS[n, tp] = rows
 
+    def exchange_start(n):
         def step(k, carry):
             peer = (tp + k) % NS
             remote(SX.at[n], SS.at[n, tp], es.at[n], er.at[n], (sp, peer)).start()
@@ -145,9 +171,9 @@
 
     loads[1].wait()
     loads[2].wait()
-    stream = ST[...].astype(F32)
+    stream = XS[mine(0)].astype(F32)
     conv = CP[...].astype(F32)
-    exchange_start(
+    exchange_set(
         0,
         columns_to_rows([
             jnp.sum(stream * stream, axis=1, keepdims=True),
@@ -179,9 +205,8 @@
     def slot_rows(p):
         return pl.ds(pl.multiple_of(p * CAP, 16), CAP)
 
-    def send_cotangent(offset):
+    def pick_cotangent(offset):
         origin = zat(offset)
-        block = mine(offset)
 
         def pick(r, carry):
             rows = pl.ds(pl.multiple_of(r * TOK, TOK), TOK)
@@ -189,6 +214,10 @@
             return carry
 
         lax.fori_loop(0, 3, pick, 0)
+
+    def send_cotangent(offset):
+        origin = zat(offset)
+        block = mine(offset)
 
         def send(p):
             remote(
@@ -199,15 +228,24 @@
         each_peer(send)
         CT[block, slot_rows(sp), :] = SC[origin, slot_rows(sp), :]
 
+    def cotangent(offset):
+        pick_cotangent(offset)
+        send_cotangent(offset)
+
+    loads[0].wait()
+    pick_cotangent(0)
+    pl.semaphore_wait(barrier, 2 * (NS - 1))
+    exchange_start(0)
+    for h in range(2):
+        for d in range(2):
+            ring_send(UP, zat, TOK // 2, ups, upr, 1, d, h)
     send_cotangent(0)
     up_take(1)
-    up_send(2)
-
     stats = exchange_end(0)
     inverse = lax.rsqrt(stats[:, 0:1] / MODEL + EPSILON)
     mean_val = stats[:, 1:2] / CHANNELS
     inv_std = lax.rsqrt(stats[:, 2:3] / CHANNELS - mean_val * mean_val + EPSILON)
-    normed = (gain_ref[...] * ST[...].astype(F32) * inverse).astype(BF16)
+    normed = (gain_ref[...] * XS[mine(0)].astype(F32) * inverse).astype(BF16)
     for r in range(3):
         rows = pl.ds(r * TOK, TOK)
         SI[rows, :] = dot(PICK[rows, :], normed, 1, 0).astype(BF16)
@@ -219,27 +257,17 @@
     each_peer(send_input)
     X[own, slot_rows(sp), :] = SI[slot_rows(sp), :]
 
-    send_cotangent(1)
-    send_cotangent(-1)
+    cotangent(1)
+    cotangent(-1)
     up_take(2)
-    up_send(3)
-    send_cotangent(2)
-    send_cotangent(-2)
-    up_take(3)
-    up_send(4)
-    send_cotangent(3)
-    send_cotangent(-3)
-
     centred = (CP[...].astype(F32) - mean_val) * inv_std
     scaled = centred * lng_ref[...]
     CEN[...] = centred
     SCL[...] = scaled
-    MO[...] = (scaled * jax.nn.sigmoid(scaled)).astype(BF16)
+    MO[...] = (scaled * jax.nn.sigmoid(scaled)).T.astype(BF16)
     G[...] = jnp.zeros_like(G)
     A[...] = jnp.zeros_like(A)
 
-    up_take(4)
-    send_cotangent(4)
     for k in range(3, 6):
         loads[k].wait()
 
@@ -252,21 +280,17 @@
     def cols(j):
         return pl.ds(pl.multiple_of(j * W, W), W)
 
-    def add_inputs(j):
-        def step(r, carry):
-            rows = pl.ds(pl.multiple_of(r * TOK, TOK), TOK)
-            G[rows, :] = G[rows, :] + dot(X[j, rows, :], WC[cols(j), :], 1, 0)
-            return carry
-
-        lax.fori_loop(0, 3, step, 0)
-
-    def add_cotangents(j):
-        def step(r, carry):
-            rows = pl.ds(pl.multiple_of(r * TOK, TOK), TOK)
-            A[rows, :] = A[rows, :] + dot(CT[j, rows, :], WD[:, cols(j)], 1, 1)
-            return carry
-
-        lax.fori_loop(0, 3, step, 0)
+    def add_inputs(blocks):
+        total = G[...]
+        for j in blocks:
+            total = total + dot(X[j], WC[cols(j), :], 1, 0)
+        G[...] = total
+
+    def add_cotangents(blocks):
+        total = A[...]
+        for j in blocks:
+            total = total + dot(CT[j], WD[:, cols(j)], 1, 1)
+        A[...] = total
 
     def hand_over(t, d, h, offset, arriving):
         j = other(offset) if arriving else mine(offset)
@@ -285,44 +309,55 @@
         ring_send(*x_ring(1, d, h))
     for h in range(2):
         hand_over(0, 0, h, 0, False).start()
-    add_inputs(own)
+    add_inputs([own])
+    cotangent(2)
+    cotangent(-2)
+    up_take(3)
+    cotangent(3)
+    cotangent(-3)
 
     def stage_offsets(t):
         return (0,) if t == 0 else ((t, -t) if t < 4 else (4,))
-
-    def x_chunks(t):
-        if t == 0:
-            return [(0, 0, 0), (0, 1, 0)]
-        return [(d, h, -t * (1 - 2 * d)) for h in range(2) for d in range(2) if active(t, d, h)]
 
     def from_sibling(t):
         for d, h, offset in x_chunks(t):
             hand_over(t, d, h, offset, True).wait_recv()
-        for offset in stage_offsets(t):
-            add_inputs(other(offset))
-
-    def cot_from_sibling(t):
-        for offset in OFFSETS[2 * t - 2 : 2 * t]:
+        add_inputs([other(offset) for offset in stage_offsets(t)])
+
+    def cot_own(offsets):
+        for offset in offsets:
+            take_many(CT.at[mine(offset), pl.ds(0, ROWS - CAP)], cs.at[zat(offset)], cr.at[zat(offset)])
+            hand_cotangent(offset, False).start()
+        add_cotangents([mine(offset) for offset in offsets])
+
+    def cot_other(offsets):
+        for offset in offsets:
             hand_cotangent(offset, True).wait_recv()
-            add_cotangents(other(offset))
-
+        add_cotangents([other(offset) for offset in offsets])
+
+    cot_stages = ((0, 1), (-1, 2, -2), (3, -3), (4,))
     for t in range(1, 5):
         for d, h, offset in x_chunks(t):
             ring_take(*x_ring(t, d, h))
             if t < 4 and active(t + 1, d, h):
                 ring_send(*x_ring(t + 1, d, h))
             hand_over(t, d, h, offset, False).start()
-        for offset in stage_offsets(t):
-            add_inputs(mine(offset))
+        if t == 1:
+            up_take(4)
+            cotangent(4)
+        if t == 3:
+            xs_send(1)
+            for h in range(2):
+                xs_hand(0, 0, h, 0, False).start()
+        if t == 4:
+            xs_take(1)
+        add_inputs([mine(offset) for offset in stage_offsets(t)])
         from_sibling(t - 1)
-        for offset in OFFSETS[2 * t - 2 : 2 * t]:
-            take_many(CT.at[mine(offset), pl.ds(0, ROWS - CAP)], cs.at[zat(offset)], cr.at[zat(offset)])
-            hand_cotangent(offset, False).start()
-            add_cotangents(mine(offset))
+        cot_own(cot_stages[t - 1])
         if t > 1:
-            cot_from_sibling(t - 1)
+            cot_other(cot_stages[t - 2])
     from_sibling(4)
-    cot_from_sibling(4)
+    cot_other(cot_stages[3])
 
     def hidden(r, carry):
         rows = pl.ds(pl.multiple_of(r * 64, 64), 64)
@@ -336,27 +371,29 @@
 
     lax.fori_loop(0, 12, hidden, 0)
 
-    def sub_rows(h, r):
-        return pl.ds(pl.multiple_of(h * HALF + r * 128, 128), 128)
-
     def for_sibling(offset):
         q = zat(offset)
         j = other(offset)
 
-        def step(r, carry):
-            rows = pl.ds(pl.multiple_of(r * TOK, TOK), TOK)
-            SB[q, rows, :] = dot(CAT[rows, :], WC[cols(j), :], 1, 1).astype(BF16)
-            return carry
-
-        lax.fori_loop(0, 3, step, 0)
+        SB[q] = dot(CAT[...], WC[cols(j), :], 1, 1).astype(BF16)
         remote(SB.at[q], SR.at[q], sbs.at[q], sbr.at[q], sibling).start()
 
     def take_sibling(offset):
         q = zat(offset)
         remote(SB.at[q], SR.at[q], sbs.at[q], sbr.at[q], sibling).wait_recv()
 
-    def chip_part(offset, rows):
-        return dot(CAT[rows, :], WC[cols(mine(offset)), :], 1, 1) + SR[zat(offset), rows, :].astype(F32)
+    def chip_part(offset):
+        q = zat(offset)
+        take_sibling(offset)
+        part = dot(CAT[...], WC[cols(mine(offset)), :], 1, 1) + SR[q].astype(F32)
+        AP[q] = part[:, 0:CH]
+        PB[q] = part[:, CH : 2 * CH].astype(BF16)
+
+        def send(p):
+            remote(PB.at[q, slot_rows(p)], RB.at[q, slot_rows(sp)], bs.at[q], br.at[q], (p, tp)).start()
+
+        each_peer(send)
+        RB[q, slot_rows(sp), :] = PB[q, slot_rows(sp), :]
 
     def rs_copy(d, k, h):
         part = pl.ds(h * HALF, HALF)
@@ -373,16 +410,45 @@
         if incoming:
             rs_copy(d, k - 1, h).wait_recv()
 
-        def step(r, carry):
-            rows = sub_rows(h, r)
-            total = chip_part(offset, rows)
-            if incoming:
-                total = total + RSR[d, k - 1, rows, :].astype(F32)
-            RSS[d, k, rows, :] = total.astype(BF16)
-            return carry
-
-        lax.fori_loop(0, 3, step, 0)
+        part = slice(h * HALF, h * HALF + HALF)
+        total = AP[zat(offset), part, :]
+        if incoming:
+            total = total + RSR[d, k - 1, part, :].astype(F32)
+        RSS[d, k, part, :] = total.astype(BF16)
         rs_copy(d, k, h).start()
+
+    def back_take(offset):
+        q = zat(offset)
+        take_many(RB.at[q, pl.ds(0, ROWS - CAP)], bs.at[q], br.at[q])
+
+    def token_part(offset, h):
+        return dot(PICK[:, h * CH : h * CH + CH], RB[zat(offset)], 0, 0)
+
+    def ts_copy(d, k, h):
+        part = pl.ds(h * CH, CH)
+        return remote(
+            TSS.at[d, k, part], TSR.at[d, k, part], tss.at[d, k, h], tsr.at[d, k, h], zdev(1 - 2 * d)
+        )
+
+    def ts_send(k, d, h):
+        total = token_part((4 - k) * (1 - 2 * d), h)
+        if k >= 1 and rs_active(k - 1, d, h):
+            ts_copy(d, k - 1, h).wait_recv()
+            total = total + TSR[d, k - 1, h * CH : h * CH + CH, :].astype(F32)
+        TSS[d, k, h * CH : h * CH + CH, :] = total.astype(BF16)
+        ts_copy(d, k, h).start()
+
+    def ts_step(k):
+        for offset in stage_offsets(4 - k):
+            back_take(offset)
+        for d, h in ((0, 1), (1, 0), (0, 0), (1, 1)):
+            if rs_active(k, d, h):
+                ts_send(k, d, h)
+
+    def rs_step(k):
+        for d, h in ((0, 1), (1, 0), (0, 0), (1, 1)):
+            if rs_active(k, d, h):
+                rs_send(k, d, h)
 
     def gradients(first_block):
         def step(b, carry):
@@ -398,35 +464,47 @@
     for_sibling(4)
     for_sibling(3)
     for_sibling(-3)
-    take_sibling(4)
-    rs_send(0, 0, 0)
-    rs_send(0, 1, 1)
+    xs_take(2)
+    chip_part(4)
+    rs_step(0)
+    chip_part(3)
+    chip_part(-3)
     for_sibling(2)
     for_sibling(-2)
-    take_sibling(3)
-    take_sibling(-3)
-    rs_send(1, 0, 1)
-    rs_send(1, 1, 0)
+    xs_take(3)
+    rs_step(1)
+    chip_part(2)
+    chip_part(-2)
     for_sibling(1)
     for_sibling(-1)
     for_sibling(0)
-    rs_send(1, 0, 0)
-    rs_send(1, 1, 1)
+    rs_step(2)
+    chip_part(1)
+    chip_part(-1)
+    chip_part(0)
+    ts_step(0)
+    xs_take(4)
     gradients(0)
-    take_sibling(2)
-    take_sibling(-2)
-    rs_send(2, 0, 1)
-    rs_send(2, 1, 0)
-    rs_send(2, 0, 0)
-    rs_send(2, 1, 1)
+    rs_step(3)
+    ts_step(1)
     gradients(4)
+    ts_step(2)
+    for h in range(2):
+        rs_copy(0, 3, h).wait_recv()
+        rs_copy(1, 3, h).wait_recv()
+
+        part = slice(h * HALF, h * HALF + HALF)
+        FIN[part, :] = (
+            AP[z, part, :] + RSR[0, 3, part, :].astype(F32) + RSR[1, 3, part, :].astype(F32)
+        ).astype(BF16)
+
+    def send_back(p):
+        remote(FIN.at[slot_rows(p)], RET.at[slot_rows(sp)], fs.at[0], fr.at[0], (p, tp)).start()
+
+    each_peer(send_back)
+    RET[slot_rows(sp), :] = FIN[slot_rows(sp), :]
     gradients(8)
-    take_sibling(1)
-    take_sibling(-1)
-    rs_send(3, 0, 1)
-    rs_send(3, 1, 0)
-    rs_send(3, 0, 0)
-    rs_send(3, 1, 1)
+    ts_step(3)
     gradients(12)
     stores = [
         pltpu.make_async_copy(GG, gg_h, ls.at[7]),
@@ -435,34 +513,22 @@
     ]
     for store in stores:
         store.start()
-    take_sibling(0)
-    for h in (1, 0):
-        rs_copy(0, 3, h).wait_recv()
-        rs_copy(1, 3, h).wait_recv()
-
-        def finish(r, carry):
-            rows = sub_rows(h, r)
-            FIN[rows, :] = (
-                chip_part(0, rows) + RSR[0, 3, rows, :].astype(F32) + RSR[1, 3, rows, :].astype(F32)
-            ).astype(BF16)
-            return carry
-
-        lax.fori_loop(0, 3, finish, 0)
-
-    def send_back(p):
-        remote(FIN.at[slot_rows(p)], RET.at[slot_rows(sp)], fs.at[0], fr.at[0], (p, tp)).start()
-
-    each_peer(send_back)
-    RET[slot_rows(sp), :] = FIN[slot_rows(sp), :]
+    back_take(0)
+    for h in range(2):
+        part = slice(h * CH, h * CH + CH)
+        total = token_part(0, h)
+        for d in range(2):
+            ts_copy(d, 3, h).wait_recv()
+            total = total + TSR[d, 3, part, :].astype(F32)
+        TB[part, CH : 2 * CH] = total
     take_many(RET.at[pl.ds(0, ROWS - CAP)], fs.at[0], fr.at[0])
-
-    gained = gain_ref[...] * dot(PICK[...], RET[...], 0, 0)
-    residual = ST[...].astype(F32)
-    exchange_start(1, columns_to_rows([jnp.sum(gained * residual, axis=1, keepdims=True)]))
-    inner = exchange_end(1)[:, 0:1] / MODEL
-    SG[own] = (
-        UP[z].astype(F32) + inverse * gained - residual * (inverse * inverse * inverse * inner)
-    ).astype(BF16)
+    TB[:, 0:CH] = dot(PICK[...], RET[...], 0, 0)
+
+    gained = gain_ref[...] * TB[...]
+    residual = XS[mine(0)].astype(F32)
+    exchange_set(1, columns_to_rows([jnp.sum(gained * residual, axis=1, keepdims=True)]))
+    exchange_start(1)
+    SG[own] = (UP[z].astype(F32) + inverse * gained).astype(BF16)
 
     def sg_ring(t, d, h):
         return (SG, mine, TOK // 2, sgs, sgr, t, d, h)
@@ -479,48 +545,55 @@
     loads[6].wait()
 
     def mix(j):
-        MB[...] = MB[...] + dot(SG[j], WO[:, cols(j)], 1, 1)
+        block = (SG[j].astype(F32) - XS[j].astype(F32) * share).astype(BF16)
+        part = dot(MO[...], block, 1, 0).astype(BF16)
+
+        @pl.when(j == sp)
+        def _():
+            GOR[sp] = part
+
+        @pl.when(j != sp)
+        def _():
+            GOS[j] = part
+            remote(GOS.at[j], GOR.at[sp], gs.at[0], gr.at[0], (j, tp)).start()
+
+        MB[...] = MB[...] + dot(block, WO[:, cols(j)], 1, 1)
 
     MB[...] = jnp.zeros_like(MB)
-    mix(own)
+
+    def mix_other(t):
+        for d, h, offset in x_chunks(t):
+            xs_hand(t, d, h, offset, True).wait_recv()
+            sg_hand(t, d, h, offset, True).wait_recv()
+        for offset in stage_offsets(t):
+            mix(other(offset))
+
     for t in range(1, 5):
         for d, h, offset in x_chunks(t):
             ring_take(*sg_ring(t, d, h))
             if t < 4 and active(t + 1, d, h):
                 ring_send(*sg_ring(t + 1, d, h))
             sg_hand(t, d, h, offset, False).start()
+        if t == 1:
+            inner = exchange_end(1)[:, 0:1] / MODEL
+            share = inverse * inverse * inverse * inner
+            mix(own)
         for offset in stage_offsets(t):
             mix(mine(offset))
-        for d, h, offset in x_chunks(t - 1):
-            sg_hand(t - 1, d, h, offset, True).wait_recv()
-        for offset in stage_offsets(t - 1):
-            mix(other(offset))
-    for d, h, offset in x_chunks(4):
-        sg_hand(4, d, h, offset, True).wait_recv()
-    mix(other(4))
+        mix_other(t - 1)
+    mix_other(4)
 
     scaled = SCL[...]
     norm_in = MB[...] * silu_slope(scaled, jax.nn.sigmoid(scaled)) * lng_ref[...]
-    exchange_start(
+    exchange_set(
         2,
         columns_to_rows([
             jnp.sum(norm_in, axis=1, keepdims=True),
             jnp.sum(norm_in * CEN[...], axis=1, keepdims=True),
         ]),
     )
-
-    def out_block(p):
-        GOS[p] = dot(MO[...], SG[p], 0, 0).astype(BF16)
-        remote(GOS.at[p], GOR.at[sp], gs.at[0], gr.at[0], (p, tp)).start()
-
-    def out_blocks(low, high):
-        def step(k, carry):
-            out_block((sp + k) % NS)
-            return carry
-
-        lax.fori_loop(low, high, step, 0)
-
-    out_blocks(1, 6)
+    exchange_start(2)
+
     sums = exchange_end(2)
     conv_back = inv_std * (
         norm_in - sums[:, 0:1] / CHANNELS - CEN[...] * (sums[:, 1:2] / CHANNELS)
@@ -533,8 +606,6 @@
         remote(HS, HALO, hs.at[0], hr.at[0], previous).start()
 
     cb_o[0:TOK, :] = conv_back
-    out_blocks(6, NS)
-    GOR[sp] = dot(MO[...], SG[sp], 0, 0).astype(BF16)
 
     @pl.when(sp < NS - 1)
     def _():
@@ -558,19 +629,23 @@
                 ring(UP, zat, TOK // 2, ups, upr, t, d, h, False).wait_send()
                 ring(*x_ring(t, d, h), False).wait_send()
                 ring(*sg_ring(t, d, h), False).wait_send()
+                ring(XS, mine, TOK // 2, sts, str_, t, d, h, False).wait_send()
     for t in range(5):
         for d, h, offset in x_chunks(t):
             hand_over(t, d, h, offset, False).wait_send()
             sg_hand(t, d, h, offset, False).wait_send()
+            xs_hand(t, d, h, offset, False).wait_send()
     for offset in OFFSETS:
         q = zat(offset)
         flush_many(SC.at[q, pl.ds(0, ROWS - CAP)], cs.at[q], cr.at[q])
         hand_cotangent(offset, False).wait_send()
+        flush_many(PB.at[q, pl.ds(0, ROWS - CAP)], bs.at[q], br.at[q])
         remote(SB.at[q], SR.at[q], sbs.at[q], sbr.at[q], sibling).wait_send()
     for k in range(4):
         for d, h in STEPS:
             if rs_active(k, d, h):
                 rs_copy(d, k, h).wait_send()
+                ts_copy(d, k, h).wait_send()
     for n in range(3):
         exchange_flush(n)
     flush_many(SI.at[pl.ds(0, ROWS - CAP)], as_.at[0], ar.at[0])
@@ -586,8 +661,8 @@
 
 
 def last_kernel(
-    gg_i, gu_i, gd_i, cb_ref, taps_ref, value_ref, gate_ref,
-    gg_o, gu_o, gd_o, vg_o, tg_o, bufs_tall, buf_wide, lsem, ssem,
+    gg_i, gu_i, gd_i, cb_ref, go_ref, taps_ref, value_ref, gate_ref,
+    gg_o, gu_o, gd_o, vg_o, tg_o, go_o, bufs_tall, buf_wide, lsem, ssem,
 ):
     pieces = []
     for a, (src, dst) in enumerate(((gg_i, gg_o), (gu_i, gu_o))):
@@ -604,6 +679,7 @@
     for i, o in zip(ins, outs):
         i.wait()
         o.start()
+    go_o[...] = go_ref[...]
     acc = jnp.zeros((TOK, CH), F32)
     for tap in range(TAPS):
         acc = acc + taps_ref[tap : tap + 1, :] * cb_ref[TAPS - 1 - tap : TAPS - 1 - tap + TOK, :]
@@ -626,7 +702,7 @@
     dma, vm = pltpu.SemaphoreType.DMA, pltpu.VMEM
     grads = [shape((MODEL, CH), F32), shape((MODEL, CH), F32), shape((CH, MODEL), F32)]
     scratch = [
-        vm((NZ, TOK, W), BF16), vm((TOK, W), BF16), vm((TOK, CH), BF16),
+        vm((NZ, TOK, W), BF16), vm((NS, TOK, W), BF16), vm((TOK, CH), BF16),
         vm((MODEL, 2 * CH), BF16), vm((CH, MODEL), BF16), vm((CH, MODEL), BF16),
         vm((ROWS, TOK), BF16), vm((ROWS, 1), F32),
         vm((ROWS, W), BF16), vm((NZ, ROWS, W), BF16),
@@ -635,10 +711,13 @@
         vm((ROWS, 2 * CH), BF16), vm((ROWS, CH), BF16),
         vm((MODEL, CH), F32), vm((MODEL, CH), F32), vm((CH, MODEL), F32),
         vm((NZ, ROWS, W), BF16), vm((NZ, ROWS, W), BF16),
-        vm((2, 4, ROWS, W), BF16), vm((2, 4, ROWS, W), BF16),
-        vm((ROWS, W), BF16), vm((ROWS, W), BF16),
+        vm((2, 4, ROWS, CH), BF16), vm((2, 4, ROWS, CH), BF16),
+        vm((NZ, ROWS, CH), BF16), vm((NZ, ROWS, CH), BF16),
+        vm((2, 4, TOK, CH), BF16), vm((2, 4, TOK, CH), BF16), vm((TOK, W), F32),
+        vm((NZ, ROWS, CH), F32),
+        vm((ROWS, CH), BF16), vm((ROWS, CH), BF16),
         vm((NS, TOK, W), BF16), vm((TOK, CH), F32),
-        vm((TOK, CH), BF16), vm((TOK, CH), F32), vm((TOK, CH), F32),
+        vm((CH, TOK), BF16), vm((TOK, CH), F32), vm((TOK, CH), F32),
         vm((32, CH), F32), vm((32, CH), F32),
         vm((NS, CH, W), BF16), vm((NS, CH, W), BF16),
         vm((3, NS, 8, TOK), F32), vm((3, 8, TOK), F32),
@@ -649,12 +728,14 @@
         dma((NZ,)), dma((NZ,)), dma((NZ,)), dma((NZ,)),
         dma((NZ,)), dma((NZ,)),
         dma((2, 4, 2)), dma((2, 4, 2)),
+        dma((NZ,)), dma((NZ,)), dma((2, 4, 2)), dma((2, 4, 2)),
+        dma((2, 4, 2)), dma((2, 4, 2)), dma((5, 2, 2)), dma((5, 2, 2)),
         dma((3,)), dma((3,)),
         dma((1,)), dma((1,)),
         dma((2, 4, 2)), dma((2, 4, 2)), dma((5, 2, 2)), dma((5, 2, 2)),
         dma((1,)), dma((1,)), dma((1,)), dma((1,)),
     ]
-    gg, gu, gd, conv_back, grad_out = pl.pallas_call(
+    gg, gu, gd, conv_back, out_sum = pl.pallas_call(
         comm_kernel,
         name="exchange",
         out_shape=grads + [shape((TOK + 32, CH), F32), shape((CH, W), F32)],
@@ -668,17 +749,17 @@
         norm_gain.reshape(1, W), routes.T, route_weights.T, ln_gain.reshape(1, CH),
         upstream, stream, w_gate[0], w_up[0], w_down[0], conv_pre, w_out,
     )
-    grad_gate, grad_up, grad_down, value_grad, gate_grad = pl.pallas_call(
+    grad_gate, grad_up, grad_down, value_grad, gate_grad, grad_out = pl.pallas_call(
         last_kernel,
         name="last",
-        out_shape=grads + [shape((TOK, CH), BF16)] * 2,
-        in_specs=[far] * 3 + [near] * 4,
-        out_specs=[far] * 3 + [near] * 2,
+        out_shape=grads + [shape((TOK, CH), BF16)] * 2 + [shape((CH, W), F32)],
+        in_specs=[far] * 3 + [near] * 5,
+        out_specs=[far] * 3 + [near] * 3,
         scratch_shapes=[
             vm((2, MODEL, CH), F32), vm((CH, MODEL), F32), dma((12,)), dma((12,)),
         ],
-        compiler_params=pltpu.CompilerParams(vmem_limit_bytes=40_000_000),
-    )(gg, gu, gd, conv_back, conv_taps, value_in, gate_in)
+        compiler_params=pltpu.CompilerParams(vmem_limit_bytes=67_000_000),
+    )(gg, gu, gd, conv_back, out_sum, conv_taps, value_in, gate_in)
     return (grad_gate[None], grad_up[None], grad_down[None], grad_out, value_grad, gate_grad)
 
 

time: 175 us -> 144 us (0.82); the launches traced: 173 us -> 144 us
  Pallas kernels: 164 us -> 143 us
  local copies, waits for them, and re-layouts: 8.02 us -> 0 us
    pallas_call x1, Pallas kernels: 160 us -> 136 us  [per_device(): pl.pallas_call(comm_kernel, name='exchange', out_shape=grads + [shape((TO...]
    unnamed x17 -> x0, local copies, waits for them, and re-layouts: 8.02 us -> none
    pallas_call x1, Pallas kernels: 3.93 us -> 7.18 us  [per_device(): pl.pallas_call(last_kernel, name='last', out_shape=grads + [shape((TOK, C...]
where the time goes in v2:
time: 144 us
  Pallas kernels  143 us (99%)
    pallas_call x1, Pallas kernels, per_device(): pl.pallas_call(comm_kernel, name='exchange', out_shape=grads + [shape((TO...  136 us
    pallas_call x1, Pallas kernels, per_device(): pl.pallas_call(last_kernel, name='last', out_shape=grads + [shape((TOK, C...  7.18 us

profile of v2, /device:TPU:17, one launch (start us, length us, event | category | flops | bytes accessed | tf_op | source)
XLA Modules:
  0.0 144.2 jit_solution(10853765559752944288)
XLA Ops:
  0.6 136.3 %exchange.1 = (f32[4096,128]{1,0:T(8,128)}, f32[4096,128]{1,0:T(8,128)}, f32[128,4096]{1,0:T(8,128)}, f32[288,128]{1,0:T(8,128)}, f32[128,256]{1,0:T(8,128)}) custom-call(f32[1,256]{1,0:T(1,128)} %bitcast.15, s32[2,256]{1,0:T(2,128)} %bitcast.13, f32[2,256]{1,0:T(2,128)} %bitcast.14, f32[1,128]{1,0:T(1,128)} %bitcast.16, bf16[256,256]{1,0:T(8,128)(2,1)} %up_h.1, ...), custom_call_target="tpu_custom_call" | custom-call | tf_op jit(solution)/shard_map/exchange/pallas_call | solution.py:738
  136.9 7.2 %last.1 = (f32[4096,128]{1,0:T(8,128)}, f32[4096,128]{1,0:T(8,128)}, f32[128,4096]{1,0:T(8,128)}, bf16[256,128]{1,0:T(8,128)(2,1)}, bf16[256,128]{1,0:T(8,128)(2,1)}, /*index=5*/f32[128,256]{1,0:T(8,128)}) custom-call(f32[4096,128]{1,0:T(8,128)} %get-tuple-element.17.gg_i, f32[4096,128]{1,0:T(8,128)} %get-tuple-element.18.gu_i, ...), custom_call_target="tpu_custom_call" | custom-call | tf_op jit(solution)/shard_map/last/pallas_call | solution.py:752

commit v3 on v2

--- a/solution.py
+++ b/solution.py
@@ -25,11 +25,13 @@
     packed = jnp.zeros((TOK, 128), F32)
     for k, column in enumerate(columns):
         packed = jnp.where(lane == k, column, packed)
-    return packed.T[0:8, :]
+    rows = packed.T[0:4, :]
+    return jnp.concatenate([rows[:, 0:128], rows[:, 128:TOK]], axis=0)
 
 
 def rows_to_columns(rows):
-    return jnp.concatenate([rows, jnp.zeros((120, TOK), F32)], axis=0).T
+    rows = jnp.concatenate([rows[0:4, :], rows[4:8, :]], axis=1)
+    return jnp.concatenate([rows, jnp.zeros((124, TOK), F32)], axis=0).T
 
 
 def silu_slope(values, logistic):
@@ -39,10 +41,10 @@
 def comm_kernel(
     gain_ref, routes_ref, rw_ref, lng_ref, up_h, st_h, wg_h, wu_h, wd_h, cp_h, wo_h,
     gg_h, gu_h, gd_h, cb_o, go_o,
-    UP, XS, CP, WC, WD, WO, PICK, SW, SI, SC, X, CT, G, A, CAT, ACT, GG, GU, GD,
-    SB, SR, RSS, RSR, PB, RB, TSS, TSR, TB, AP, FIN, RET, SG, MB, MO, CEN, SCL, HS, HALO, GOS, GOR, SS, SX,
+    UP, ST, CP, WC, WD, WO, PICK, SW, SI, SC, X, CT, G, A, CAT, ACT, GG, GU, GD,
+    SB, SR, RSS, RSR, PB, RB, TSS, TSR, AP, RK, RC, KS, KR, FIN, RET, SG, MB, MO, CEN, SCL, HS, HALO, GOS, GOR, SS, SX,
     ls, ups, upr, xs, xr, dxs, dxr, as_, ar, cs, cr, dcs, dcr, sbs, sbr, rss, rsr, bs, br, tss, tsr,
-    sts, str_, dts, dtr, es, er, fs, fr, sgs, sgr, dgs, dgr, gs, gr, hs, hr,
+    ks, kr, es, er, fs, fr, sgs, sgr, dgs, dgr, gs, gr, hs, hr,
 ):
     sp = lax.axis_index("sp")
     tp = lax.axis_index("tp")
@@ -85,7 +87,7 @@
     lax.fori_loop(1, NS, greet, 0)
     loads = [
         pltpu.make_async_copy(up_h, UP.at[z], ls.at[0]),
-        pltpu.make_async_copy(st_h, XS.at[mine(0)], ls.at[1]),
+        pltpu.make_async_copy(st_h, ST, ls.at[1]),
         pltpu.make_async_copy(cp_h, CP, ls.at[2]),
         pltpu.make_async_copy(wg_h, WC.at[:, pl.ds(0, CH)], ls.at[3]),
         pltpu.make_async_copy(wu_h, WC.at[:, pl.ds(CH, CH)], ls.at[4]),
@@ -109,36 +111,10 @@
     def ring_take(*args):
         ring(*args, True).wait_recv()
 
-    def halves_ring(buf, ssem, rsem):
-        def send(t):
-            for h in range(2):
-                for d in range(2):
-                    if active(t, d, h):
-                        ring_send(buf, mine, TOK // 2, ssem, rsem, t, d, h)
-
-        def hand(t, d, h, offset, arriving, hs_, hr_):
-            j = other(offset) if arriving else mine(offset)
-            block = buf.at[j, pl.ds(h * (TOK // 2), TOK // 2)]
-            return remote(block, block, hs_.at[t, d, h], hr_.at[t, d, h], sibling)
-
-        return send, hand
-
     def x_chunks(t):
         if t == 0:
             return [(0, 0, 0), (0, 1, 0)]
         return [(d, h, -t * (1 - 2 * d)) for h in range(2) for d in range(2) if active(t, d, h)]
-
-    xs_send, xs_hand_ = halves_ring(XS, sts, str_)
-
-    def xs_hand(t, d, h, offset, arriving):
-        return xs_hand_(t, d, h, offset, arriving, dts, dtr)
-
-    def xs_take(t):
-        for d, h, offset in x_chunks(t):
-            ring_take(XS, mine, TOK // 2, sts, str_, t, d, h)
-            if t < 4 and active(t + 1, d, h):
-                ring_send(XS, mine, TOK // 2, sts, str_, t + 1, d, h)
-            xs_hand(t, d, h, offset, False).start()
 
     def up_take(t):
         for h in range(2):
@@ -171,7 +147,7 @@
 
     loads[1].wait()
     loads[2].wait()
-    stream = XS[mine(0)].astype(F32)
+    stream = ST[...].astype(F32)
     conv = CP[...].astype(F32)
     exchange_set(
         0,
@@ -190,8 +166,12 @@
         lax.broadcasted_iota(jnp.int32, (TOK, TOK), 0) < lax.broadcasted_iota(jnp.int32, (TOK, TOK), 1)
     ).astype(F32).astype(BF16)
     rank = dot((hit0 + hit1).astype(BF16), earlier, 1, 0)
-    slot0 = first * CAP + jnp.sum(hit0 * rank, axis=0, keepdims=True).astype(jnp.int32)
-    slot1 = second * CAP + jnp.sum(hit1 * rank, axis=0, keepdims=True).astype(jnp.int32)
+    rank0 = jnp.sum(hit0 * rank, axis=0, keepdims=True).astype(jnp.int32)
+    rank1 = jnp.sum(hit1 * rank, axis=0, keepdims=True).astype(jnp.int32)
+    RK[0:1, :] = rank0
+    RK[1:2, :] = rank1
+    slot0 = first * CAP + rank0
+    slot1 = second * CAP + rank1
     for r in range(3):
         slots = lax.broadcasted_iota(jnp.int32, (TOK, TOK), 0) + r * TOK
         at0, at1 = slots == slot0, slots == slot1
@@ -240,12 +220,11 @@
         for d in range(2):
             ring_send(UP, zat, TOK // 2, ups, upr, 1, d, h)
     send_cotangent(0)
-    up_take(1)
     stats = exchange_end(0)
     inverse = lax.rsqrt(stats[:, 0:1] / MODEL + EPSILON)
     mean_val = stats[:, 1:2] / CHANNELS
     inv_std = lax.rsqrt(stats[:, 2:3] / CHANNELS - mean_val * mean_val + EPSILON)
-    normed = (gain_ref[...] * XS[mine(0)].astype(F32) * inverse).astype(BF16)
+    normed = (gain_ref[...] * ST[...].astype(F32) * inverse).astype(BF16)
     for r in range(3):
         rows = pl.ds(r * TOK, TOK)
         SI[rows, :] = dot(PICK[rows, :], normed, 1, 0).astype(BF16)
@@ -257,6 +236,7 @@
     each_peer(send_input)
     X[own, slot_rows(sp), :] = SI[slot_rows(sp), :]
 
+    up_take(1)
     cotangent(1)
     cotangent(-1)
     up_take(2)
@@ -345,12 +325,6 @@
         if t == 1:
             up_take(4)
             cotangent(4)
-        if t == 3:
-            xs_send(1)
-            for h in range(2):
-                xs_hand(0, 0, h, 0, False).start()
-        if t == 4:
-            xs_take(1)
         add_inputs([mine(offset) for offset in stage_offsets(t)])
         from_sibling(t - 1)
         cot_own(cot_stages[t - 1])
@@ -365,11 +339,54 @@
         logistic = jax.nn.sigmoid(gate)
         silu = gate * logistic
         ACT[rows, :] = (silu * upper).astype(BF16)
-        CAT[rows, 0:CH] = (back * upper * silu_slope(gate, logistic)).astype(BF16)
-        CAT[rows, CH : 2 * CH] = (back * silu).astype(BF16)
+        gate_back = (back * upper * silu_slope(gate, logistic)).astype(BF16)
+        upper_back = (back * silu).astype(BF16)
+        CAT[rows, 0:CH] = gate_back
+        CAT[rows, CH : 2 * CH] = upper_back
         return carry
 
     lax.fori_loop(0, 12, hidden, 0)
+
+    def send_sums():
+        def row_sums(r, carry):
+            rows = pl.ds(pl.multiple_of(r * 64, 64), 64)
+            RC[rows, :] = jnp.sum(CAT[rows, :].astype(F32) * G[rows, :], axis=1, keepdims=True)
+            return carry
+
+        lax.fori_loop(0, 12, row_sums, 0)
+        slot_lane = lax.broadcasted_iota(jnp.int32, (CAP, 128), 0) == lax.broadcasted_iota(
+            jnp.int32, (CAP, 128), 1
+        )
+        top = lax.broadcasted_iota(jnp.int32, (8, 128), 0) == 0
+        for p in range(NS):
+            row = jnp.sum(jnp.where(slot_lane, RC[p * CAP : p * CAP + CAP, :], 0.0), axis=0, keepdims=True)
+            KS[p] = jnp.where(top, row, 0.0)
+
+        def send(p):
+            remote(KS.at[p], KR.at[sp], ks.at[0], kr.at[0], (p, tp)).start()
+
+        each_peer(send)
+        KR[sp] = KS[sp]
+
+    def inner_sums():
+        take_many(KR.at[pl.ds(0, NS - 1)], ks.at[0], kr.at[0])
+        by_slot = jnp.sum(KR[...], axis=1)
+        names = lax.broadcasted_iota(jnp.int32, (NS, TOK), 0)
+        ranks = lax.broadcasted_iota(jnp.int32, (128, TOK), 0)
+        total = jnp.zeros((1, TOK), F32)
+        for k in range(2):
+            picked = lax.dot_general(
+                by_slot, (ranks == RK[k : k + 1, :]).astype(F32), (((1,), (0,)), ((), ())),
+                precision=lax.Precision.HIGHEST, preferred_element_type=F32,
+            )
+            total = total + jnp.sum(
+                jnp.where(names == routes_ref[k : k + 1, :], picked, 0.0), axis=0, keepdims=True
+            )
+        row = lax.broadcasted_iota(jnp.int32, (8, 128), 0)
+        exchange_set(
+            1, jnp.where(row == 0, total[:, 0:128], jnp.where(row == 4, total[:, 128:TOK], 0.0))
+        )
+        exchange_start(1)
 
     def for_sibling(offset):
         q = zat(offset)
@@ -464,14 +481,13 @@
     for_sibling(4)
     for_sibling(3)
     for_sibling(-3)
-    xs_take(2)
     chip_part(4)
     rs_step(0)
+    send_sums()
     chip_part(3)
     chip_part(-3)
     for_sibling(2)
     for_sibling(-2)
-    xs_take(3)
     rs_step(1)
     chip_part(2)
     chip_part(-2)
@@ -479,16 +495,15 @@
     for_sibling(-1)
     for_sibling(0)
     rs_step(2)
+    inner_sums()
+    ts_step(0)
     chip_part(1)
     chip_part(-1)
-    chip_part(0)
-    ts_step(0)
-    xs_take(4)
     gradients(0)
     rs_step(3)
+    chip_part(0)
     ts_step(1)
     gradients(4)
-    ts_step(2)
     for h in range(2):
         rs_copy(0, 3, h).wait_recv()
         rs_copy(1, 3, h).wait_recv()
@@ -503,49 +518,45 @@
 
     each_peer(send_back)
     RET[slot_rows(sp), :] = FIN[slot_rows(sp), :]
+    ts_step(2)
     gradients(8)
     ts_step(3)
-    gradients(12)
-    stores = [
-        pltpu.make_async_copy(GG, gg_h, ls.at[7]),
-        pltpu.make_async_copy(GU, gu_h, ls.at[8]),
-        pltpu.make_async_copy(GD, gd_h, ls.at[9]),
-    ]
-    for store in stores:
-        store.start()
+    def sg_ring(t, d, h, arriving):
+        sign = 1 - 2 * d
+        block = SG.at[mine(-sign * (t if arriving else t - 1)), :, pl.ds(h * CH, CH)]
+        return remote(block, block, sgs.at[d, t - 1, h], sgr.at[d, t - 1, h], zdev(sign))
+
+    def sg_hand(t, d, h, offset, arriving):
+        block = SG.at[other(offset) if arriving else mine(offset), :, pl.ds(h * CH, CH)]
+        return remote(block, block, dgs.at[t, d, h], dgr.at[t, d, h], sibling)
+
+    def sg_first(h, token_back):
+        part = slice(h * CH, h * CH + CH)
+        SG[own, :, part] = (
+            UP[z, :, part].astype(F32)
+            + inverse * gain_ref[:, part] * token_back
+            - ST[:, part].astype(F32) * share
+        ).astype(BF16)
+        for d in range(2):
+            sg_ring(1, d, h, False).start()
+        sg_hand(0, 0, h, 0, False).start()
+
+    share = inverse * inverse * (exchange_end(1)[:, 0:1] / MODEL)
+    take_many(RET.at[pl.ds(0, ROWS - CAP)], fs.at[0], fr.at[0])
+    sg_first(0, dot(PICK[...], RET[...], 0, 0))
     back_take(0)
+    finals = []
     for h in range(2):
-        part = slice(h * CH, h * CH + CH)
         total = token_part(0, h)
         for d in range(2):
             ts_copy(d, 3, h).wait_recv()
-            total = total + TSR[d, 3, part, :].astype(F32)
-        TB[part, CH : 2 * CH] = total
-    take_many(RET.at[pl.ds(0, ROWS - CAP)], fs.at[0], fr.at[0])
-    TB[:, 0:CH] = dot(PICK[...], RET[...], 0, 0)
-
-    gained = gain_ref[...] * TB[...]
-    residual = XS[mine(0)].astype(F32)
-    exchange_set(1, columns_to_rows([jnp.sum(gained * residual, axis=1, keepdims=True)]))
-    exchange_start(1)
-    SG[own] = (UP[z].astype(F32) + inverse * gained).astype(BF16)
-
-    def sg_ring(t, d, h):
-        return (SG, mine, TOK // 2, sgs, sgr, t, d, h)
-
-    def sg_hand(t, d, h, offset, arriving):
-        j = other(offset) if arriving else mine(offset)
-        block = SG.at[j, pl.ds(h * (TOK // 2), TOK // 2)]
-        return remote(block, block, dgs.at[t, d, h], dgr.at[t, d, h], sibling)
-
-    for d, h in STEPS:
-        ring_send(*sg_ring(1, d, h))
-    for h in range(2):
-        sg_hand(0, 0, h, 0, False).start()
+            total = total + TSR[d, 3, h * CH : h * CH + CH, :].astype(F32)
+        finals.append(total)
+    sg_first(1, jnp.concatenate(finals, axis=0))
     loads[6].wait()
 
     def mix(j):
-        block = (SG[j].astype(F32) - XS[j].astype(F32) * share).astype(BF16)
+        block = SG[j]
         part = dot(MO[...], block, 1, 0).astype(BF16)
 
         @pl.when(j == sp)
@@ -560,24 +571,20 @@
         MB[...] = MB[...] + dot(block, WO[:, cols(j)], 1, 1)
 
     MB[...] = jnp.zeros_like(MB)
+    mix(own)
 
     def mix_other(t):
         for d, h, offset in x_chunks(t):
-            xs_hand(t, d, h, offset, True).wait_recv()
             sg_hand(t, d, h, offset, True).wait_recv()
         for offset in stage_offsets(t):
             mix(other(offset))
 
     for t in range(1, 5):
         for d, h, offset in x_chunks(t):
-            ring_take(*sg_ring(t, d, h))
+            sg_ring(t, d, h, True).wait_recv()
             if t < 4 and active(t + 1, d, h):
-                ring_send(*sg_ring(t + 1, d, h))
+                sg_ring(t + 1, d, h, False).start()
             sg_hand(t, d, h, offset, False).start()
-        if t == 1:
-            inner = exchange_end(1)[:, 0:1] / MODEL
-            share = inverse * inverse * inverse * inner
-            mix(own)
         for offset in stage_offsets(t):
             mix(mine(offset))
         mix_other(t - 1)
@@ -594,6 +601,14 @@
     )
     exchange_start(2)
 
+    gradients(12)
+    stores = [
+        pltpu.make_async_copy(GG, gg_h, ls.at[7]),
+        pltpu.make_async_copy(GU, gu_h, ls.at[8]),
+        pltpu.make_async_copy(GD, gd_h, ls.at[9]),
+    ]
+    for store in stores:
+        store.start()
     sums = exchange_end(2)
     conv_back = inv_std * (
         norm_in - sums[:, 0:1] / CHANNELS - CEN[...] * (sums[:, 1:2] / CHANNELS)
@@ -628,13 +643,11 @@
             if active(t, d, h):
                 ring(UP, zat, TOK // 2, ups, upr, t, d, h, False).wait_send()
                 ring(*x_ring(t, d, h), False).wait_send()
-                ring(*sg_ring(t, d, h), False).wait_send()
-                ring(XS, mine, TOK // 2, sts, str_, t, d, h, False).wait_send()
+                sg_ring(t, d, h, False).wait_send()
     for t in range(5):
         for d, h, offset in x_chunks(t):
             hand_over(t, d, h, offset, False).wait_send()
             sg_hand(t, d, h, offset, False).wait_send()
-            xs_hand(t, d, h, offset, False).wait_send()
     for offset in OFFSETS:
         q = zat(offset)
         flush_many(SC.at[q, pl.ds(0, ROWS - CAP)], cs.at[q], cr.at[q])
@@ -648,6 +661,7 @@
                 ts_copy(d, k, h).wait_send()
     for n in range(3):
         exchange_flush(n)
+    flush_many(KS.at[pl.ds(0, NS - 1)], ks.at[0], kr.at[0])
     flush_many(SI.at[pl.ds(0, ROWS - CAP)], as_.at[0], ar.at[0])
     flush_many(FIN.at[pl.ds(0, ROWS - CAP)], fs.at[0], fr.at[0])
     flush_many(GOS.at[pl.ds(0, NS - 1)], gs.at[0], gr.at[0])
@@ -702,7 +716,7 @@
     dma, vm = pltpu.SemaphoreType.DMA, pltpu.VMEM
     grads = [shape((MODEL, CH), F32), shape((MODEL, CH), F32), shape((CH, MODEL), F32)]
     scratch = [
-        vm((NZ, TOK, W), BF16), vm((NS, TOK, W), BF16), vm((TOK, CH), BF16),
+        vm((NZ, TOK, W), BF16), vm((TOK, W), BF16), vm((TOK, CH), BF16),
         vm((MODEL, 2 * CH), BF16), vm((CH, MODEL), BF16), vm((CH, MODEL), BF16),
         vm((ROWS, TOK), BF16), vm((ROWS, 1), F32),
         vm((ROWS, W), BF16), vm((NZ, ROWS, W), BF16),
@@ -713,14 +727,15 @@
         vm((NZ, ROWS, W), BF16), vm((NZ, ROWS, W), BF16),
         vm((2, 4, ROWS, CH), BF16), vm((2, 4, ROWS, CH), BF16),
         vm((NZ, ROWS, CH), BF16), vm((NZ, ROWS, CH), BF16),
-        vm((2, 4, TOK, CH), BF16), vm((2, 4, TOK, CH), BF16), vm((TOK, W), F32),
-        vm((NZ, ROWS, CH), F32),
+        vm((2, 4, TOK, CH), BF16), vm((2, 4, TOK, CH), BF16),
+        vm((NZ, ROWS, CH), F32), vm((8, TOK), jnp.int32), vm((ROWS, 1), F32),
+        vm((NS, 8, 128), F32), vm((NS, 8, 128), F32),
         vm((ROWS, CH), BF16), vm((ROWS, CH), BF16),
         vm((NS, TOK, W), BF16), vm((TOK, CH), F32),
         vm((CH, TOK), BF16), vm((TOK, CH), F32), vm((TOK, CH), F32),
         vm((32, CH), F32), vm((32, CH), F32),
         vm((NS, CH, W), BF16), vm((NS, CH, W), BF16),
-        vm((3, NS, 8, TOK), F32), vm((3, 8, TOK), F32),
+        vm((3, NS, 8, 128), F32), vm((3, 8, 128), F32),
         dma((10,)),
         dma((2, 4, 2)), dma((2, 4, 2)), dma((2, 4, 2)), dma((2, 4, 2)),
         dma((5, 2, 2)), dma((5, 2, 2)),
@@ -729,7 +744,7 @@
         dma((NZ,)), dma((NZ,)),
         dma((2, 4, 2)), dma((2, 4, 2)),
         dma((NZ,)), dma((NZ,)), dma((2, 4, 2)), dma((2, 4, 2)),
-        dma((2, 4, 2)), dma((2, 4, 2)), dma((5, 2, 2)), dma((5, 2, 2)),
+        dma((1,)), dma((1,)),
         dma((3,)), dma((3,)),
         dma((1,)), dma((1,)),
         dma((2, 4, 2)), dma((2, 4, 2)), dma((5, 2, 2)), dma((5, 2, 2)),

time: 144 us -> 134 us (0.931)
  Pallas kernels: 143 us -> 133 us
    pallas_call x1, Pallas kernels: 136 us -> 126 us  [per_device(): pl.pallas_call(comm_kernel, name='exchange', out_shape=grads + [shape((TO...]
where the time goes in v3:
time: 134 us
  Pallas kernels  133 us (99%)
    pallas_call x1, Pallas kernels, per_device(): pl.pallas_call(comm_kernel, name='exchange', out_shape=grads + [shape((TO...  126 us
    pallas_call x1, Pallas kernels, per_device(): pl.pallas_call(last_kernel, name='last', out_shape=grads + [shape((TOK, C...  7.18 us

profile of v3, /device:TPU:17, one launch (start us, length us, event | category | flops | bytes accessed | tf_op | source)
XLA Modules:
  0.0 133.8 jit_solution(12246170543992664174)
XLA Ops:
  0.6 125.8 %exchange.1 = (f32[4096,128]{1,0:T(8,128)}, f32[4096,128]{1,0:T(8,128)}, f32[128,4096]{1,0:T(8,128)}, f32[288,128]{1,0:T(8,128)}, f32[128,256]{1,0:T(8,128)}) custom-call(f32[1,256]{1,0:T(1,128)} %bitcast.15, s32[2,256]{1,0:T(2,128)} %bitcast.13, f32[2,256]{1,0:T(2,128)} %bitcast.14, f32[1,128]{1,0:T(1,128)} %bitcast.16, bf16[256,256]{1,0:T(8,128)(2,1)} %up_h.1, ...), custom_call_target="tpu_custom_call" | custom-call | tf_op jit(solution)/shard_map/exchange/pallas_call | solution.py:753
  126.4 7.2 %last.1 = (f32[4096,128]{1,0:T(8,128)}, f32[4096,128]{1,0:T(8,128)}, f32[128,4096]{1,0:T(8,128)}, bf16[256,128]{1,0:T(8,128)(2,1)}, bf16[256,128]{1,0:T(8,128)(2,1)}, /*index=5*/f32[128,256]{1,0:T(8,128)}) custom-call(f32[4096,128]{1,0:T(8,128)} %get-tuple-element.17.gg_i, f32[4096,128]{1,0:T(8,128)} %get-tuple-element.18.gu_i, ...), custom_call_target="tpu_custom_call" | custom-call | tf_op jit(solution)/shard_map/last/pallas_call | solution.py:767

commit v4 on v3

--- a/solution.py
+++ b/solution.py
@@ -188,12 +188,7 @@
     def pick_cotangent(offset):
         origin = zat(offset)
 
-        def pick(r, carry):
-            rows = pl.ds(pl.multiple_of(r * TOK, TOK), TOK)
-            SC[origin, rows, :] = (dot(PICK[rows, :], UP[origin], 1, 0) * SW[rows, :]).astype(BF16)
-            return carry
-
-        lax.fori_loop(0, 3, pick, 0)
+        SC[origin] = (dot(PICK[...], UP[origin], 1, 0) * SW[...]).astype(BF16)
 
     def send_cotangent(offset):
         origin = zat(offset)
@@ -237,8 +232,6 @@
     X[own, slot_rows(sp), :] = SI[slot_rows(sp), :]
 
     up_take(1)
-    cotangent(1)
-    cotangent(-1)
     up_take(2)
     centred = (CP[...].astype(F32) - mean_val) * inv_std
     scaled = centred * lng_ref[...]
@@ -290,6 +283,8 @@
     for h in range(2):
         hand_over(0, 0, h, 0, False).start()
     add_inputs([own])
+    cotangent(1)
+    cotangent(-1)
     cotangent(2)
     cotangent(-2)
     up_take(3)
@@ -483,7 +478,6 @@
     for_sibling(-3)
     chip_part(4)
     rs_step(0)
-    send_sums()
     chip_part(3)
     chip_part(-3)
     for_sibling(2)
@@ -495,12 +489,13 @@
     for_sibling(-1)
     for_sibling(0)
     rs_step(2)
-    inner_sums()
+    send_sums()
     ts_step(0)
     chip_part(1)
     chip_part(-1)
     gradients(0)
     rs_step(3)
+    inner_sums()
     chip_part(0)
     ts_step(1)
     gradients(4)
@@ -521,10 +516,11 @@
     ts_step(2)
     gradients(8)
     ts_step(3)
-    def sg_ring(t, d, h, arriving):
+    def sg_ring(t, d, h, r, arriving):
         sign = 1 - 2 * d
-        block = SG.at[mine(-sign * (t if arriving else t - 1)), :, pl.ds(h * CH, CH)]
-        return remote(block, block, sgs.at[d, t - 1, h], sgr.at[d, t - 1, h], zdev(sign))
+        j = mine(-sign * (t if arriving else t - 1))
+        block = SG.at[j, pl.ds(r * CH, CH), pl.ds(h * CH, CH)]
+        return remote(block, block, sgs.at[d, t - 1, h, r], sgr.at[d, t - 1, h, r], zdev(sign))
 
     def sg_hand(t, d, h, offset, arriving):
         block = SG.at[other(offset) if arriving else mine(offset), :, pl.ds(h * CH, CH)]
@@ -537,8 +533,9 @@
             + inverse * gain_ref[:, part] * token_back
             - ST[:, part].astype(F32) * share
         ).astype(BF16)
-        for d in range(2):
-            sg_ring(1, d, h, False).start()
+        for r in range(2):
+            for d in range(2):
+                sg_ring(1, d, h, r, False).start()
         sg_hand(0, 0, h, 0, False).start()
 
     share = inverse * inverse * (exchange_end(1)[:, 0:1] / MODEL)
@@ -580,11 +577,15 @@
             mix(other(offset))
 
     for t in range(1, 5):
-        for d, h, offset in x_chunks(t):
-            sg_ring(t, d, h, True).wait_recv()
-            if t < 4 and active(t + 1, d, h):
-                sg_ring(t + 1, d, h, False).start()
-            sg_hand(t, d, h, offset, False).start()
+        for h in range(2):
+            here = [(d, offset) for d, g, offset in x_chunks(t) if g == h]
+            for r in range(2):
+                for d, _ in here:
+                    sg_ring(t, d, h, r, True).wait_recv()
+                    if t < 4 and active(t + 1, d, h):
+                        sg_ring(t + 1, d, h, r, False).start()
+            for d, offset in here:
+                sg_hand(t, d, h, offset, False).start()
         for offset in stage_offsets(t):
             mix(mine(offset))
         mix_other(t - 1)
@@ -643,7 +644,8 @@
             if active(t, d, h):
                 ring(UP, zat, TOK // 2, ups, upr, t, d, h, False).wait_send()
                 ring(*x_ring(t, d, h), False).wait_send()
-                sg_ring(t, d, h, False).wait_send()
+                for r in range(2):
+                    sg_ring(t, d, h, r, False).wait_send()
     for t in range(5):
         for d, h, offset in x_chunks(t):
             hand_over(t, d, h, offset, False).wait_send()
@@ -747,7 +749,7 @@
         dma((1,)), dma((1,)),
         dma((3,)), dma((3,)),
         dma((1,)), dma((1,)),
-        dma((2, 4, 2)), dma((2, 4, 2)), dma((5, 2, 2)), dma((5, 2, 2)),
+        dma((2, 4, 2, 2)), dma((2, 4, 2, 2)), dma((5, 2, 2)), dma((5, 2, 2)),
         dma((1,)), dma((1,)), dma((1,)), dma((1,)),
     ]
     gg, gu, gd, conv_back, out_sum = pl.pallas_call(

time: 134 us -> 132 us (0.985)
  Pallas kernels: 133 us -> 131 us
    pallas_call x1, Pallas kernels: 126 us -> 124 us  [per_device(): pl.pallas_call(comm_kernel, name='exchange', out_shape=grads + [shape((TO...]
where the time goes in v4:
time: 132 us
  Pallas kernels  131 us (99%)
    pallas_call x1, Pallas kernels, per_device(): pl.pallas_call(comm_kernel, name='exchange', out_shape=grads + [shape((TO...  124 us
    pallas_call x1, Pallas kernels, per_device(): pl.pallas_call(last_kernel, name='last', out_shape=grads + [shape((TOK, C...  7.18 us

profile of v4, /device:TPU:17, one launch (start us, length us, event | category | flops | bytes accessed | tf_op | source)
XLA Modules:
  0.0 132.2 jit_solution(14500440122978661966)
XLA Ops:
  0.6 124.3 %exchange.1 = (f32[4096,128]{1,0:T(8,128)}, f32[4096,128]{1,0:T(8,128)}, f32[128,4096]{1,0:T(8,128)}, f32[288,128]{1,0:T(8,128)}, f32[128,256]{1,0:T(8,128)}) custom-call(f32[1,256]{1,0:T(1,128)} %bitcast.15, s32[2,256]{1,0:T(2,128)} %bitcast.13, f32[2,256]{1,0:T(2,128)} %bitcast.14, f32[1,128]{1,0:T(1,128)} %bitcast.16, bf16[256,256]{1,0:T(8,128)(2,1)} %up_h.1, ...), custom_call_target="tpu_custom_call" | custom-call | tf_op jit(solution)/shard_map/exchange/pallas_call | solution.py:755
  124.9 7.2 %last.1 = (f32[4096,128]{1,0:T(8,128)}, f32[4096,128]{1,0:T(8,128)}, f32[128,4096]{1,0:T(8,128)}, bf16[256,128]{1,0:T(8,128)(2,1)}, bf16[256,128]{1,0:T(8,128)(2,1)}, /*index=5*/f32[128,256]{1,0:T(8,128)}) custom-call(f32[4096,128]{1,0:T(8,128)} %get-tuple-element.17.gg_i, f32[4096,128]{1,0:T(8,128)} %get-tuple-element.18.gu_i, ...), custom_call_target="tpu_custom_call" | custom-call | tf_op jit(solution)/shard_map/last/pallas_call | solution.py:769
